TPU v7x, 768 devices: a whole 4x8x12 slice. The times are simulated.
768 devices in a mesh: sp: 96 (over z, y), tp: 8 (over x, core).
Axes of the slice: x: 4, y: 8, z: 12, core: 2. Of those that a mesh axis runs over, the one named last changes fastest.
Arguments:
- queries: bfloat16 [1, 24576, 2048], P(None, 'sp', 'tp'), may hold values from -5 to 5
- key_vectors: bfloat16 [1, 24576, 2048], P(None, 'sp', 'tp'), may hold values from -5 to 5
- value_vectors: bfloat16 [1, 24576, 2048], P(None, 'sp', 'tp'), may hold values from -40 to 40
- cotangent: bfloat16 [1, 24576, 2048], P(None, 'sp', 'tp'), may hold values from -6 to 6
- out_gain: bfloat16 [2048], P('tp'), may hold values from 0.099609375 to 1.8984375
- rel_table: bfloat16 [16, 320], P('tp'), may hold values from -4 to 4
Outputs:
- grad_queries: bfloat16 [1, 24576, 2048], P(None, 'sp', 'tp')
- grad_keys: bfloat16 [1, 24576, 2048], P(None, 'sp', 'tp')
- grad_values: bfloat16 [1, 24576, 2048], P(None, 'sp', 'tp')
- grad_table: float32 [16, 320], P('tp')
All inputs are finite; a program needn't handle non-finite values.
Results may differ from a plain program's by a relative error of at most 0.0071.
Values may be sent and summed in bfloat16 or wider, within the bound.
No kernel may reach another device: no remote copies, remote signals or barrier semaphores. Data moves between devices by JAX's collectives and lax.ppermute only.
A program may use at most 32 MiB of HBM per device.

v0:
```python
import math

import jax
import jax.numpy as jnp
from jax import lax
from jax.sharding import Mesh
from jax.sharding import PartitionSpec as P

HEAD_DIM = 128
SEG = 64
LEFT = 4
MAX_REL = 256
SP = ("sp_0", "sp_1")


epsilon = 1e-06
masked_value = -1e30


def passed_along(block, axis, distance):
    devices = range(lax.axis_size(axis))
    route = [(i - distance, i) for i in devices if i - distance in devices]
    return lax.ppermute(block, axis, route)


def sent_to_all(x, axis):
    copies = jnp.broadcast_to(x, (lax.axis_size(axis), *x.shape))
    return lax.all_to_all(copies, axis, split_axis=0, concat_axis=0, tiled=True)


def taken_together(x, axis):
    everything = sent_to_all(x, axis)
    return jnp.sum(everything, axis=0)


def packed_total(arrays, axis):
    ravelled, at, finished = (jnp.concatenate([a.reshape(-1) for a in arrays]), 0, [])
    running = taken_together(ravelled, axis)
    for a in arrays:
        finished.append(running[at : at + a.size].reshape(a.shape))
        at += a.size
    return tuple(finished)


def one_axis_at_a_time(x, axes):
    for axis in axes:
        x = lax.psum(x, axis)
    return x


def flat_bias(table_rows):
    band_width = (LEFT + 1) * SEG
    extra_cols = LEFT * SEG + SEG - 1 - MAX_REL
    extended = jnp.concatenate(
        [table_rows, jnp.broadcast_to(table_rows[:, -1:], (table_rows.shape[0], extra_cols))],
        axis=1,
    )
    hankel = jnp.stack([extended[:, offset : offset + band_width] for offset in range(SEG)], axis=1)
    return hankel[:, :, ::-1]


def as_segments(array):
    return array.reshape(
        array.shape[0], array.shape[1] // SEG, SEG, array.shape[2] // HEAD_DIM, HEAD_DIM
    )


def band_products(left_seg, right_all, seg_count, offsets):
    return jnp.concatenate(
        [
            jnp.einsum(
                "bcqhd,bckhd->bhcqk",
                left_seg,
                right_all[:, offset : offset + seg_count],
                preferred_element_type=jnp.float32,
            )
            for offset in range(offsets)
        ],
        axis=-1,
    )


def band_slice(weights, offset):
    return weights[..., offset * SEG : (offset + 1) * SEG]


def key_terms(weights, rows_seg, offset):
    return jnp.einsum(
        "bhcqk,bcqhd->bckhd",
        band_slice(weights, offset),
        rows_seg,
        preferred_element_type=jnp.float32,
    )


def place(blocks, length):
    result = None
    for begin_at, block_rows in blocks:
        padded = jnp.pad(
            block_rows,
            ((0, 0), (begin_at, length - begin_at - block_rows.shape[1]), (0, 0), (0, 0), (0, 0)),
        )
        result = padded if result is None else result + padded
    return result


def at_tail(own_rows, extra_rows):
    return own_rows + extra_rows


def on_device(queries, key_vectors, value_vectors, cotangent, out_gain, rel_table):
    seq_count, row_count, width_dev = queries.shape
    seg_count = row_count // SEG
    band_len = LEFT + 1
    scale_root = math.sqrt(HEAD_DIM)
    prior_keys, prior_values = passed_along((key_vectors, value_vectors), SP, 1)
    key_all = as_segments(jnp.concatenate([prior_keys, key_vectors], axis=1))
    value_all = as_segments(jnp.concatenate([prior_values, value_vectors], axis=1))
    query_seg = as_segments(queries)
    seg_ids = lax.axis_index(SP) * seg_count + jnp.arange(seg_count)
    visible = seg_ids[:, None] - LEFT + jnp.arange(band_len)[None, :] >= 0
    visible = jnp.repeat(visible, SEG, axis=1)
    pos_bias, pullback = jax.vjp(flat_bias, rel_table.astype(jnp.float32))
    scores = (
        band_products(query_seg, key_all, seg_count, band_len) / scale_root
        + pos_bias[None, :, None]
    )
    scores = jnp.where(visible[None, None, :, None, :], scores, masked_value)
    row_max = jnp.max(scores, axis=-1, keepdims=True)
    shifted = jnp.exp(scores - row_max)
    row_total = jnp.sum(shifted, axis=-1, keepdims=True)
    probability = shifted / row_total
    prob_low = probability.astype(jnp.bfloat16)
    attended = sum(
        (
            jnp.einsum(
                "bhcqk,bckhd->bcqhd",
                band_slice(prob_low, offset),
                value_all[:, offset : offset + seg_count],
                preferred_element_type=jnp.float32,
            )
            for offset in range(band_len)
        )
    )
    attended = attended.reshape(seq_count, row_count, width_dev)
    scaled = cotangent.astype(jnp.float32) * out_gain.astype(jnp.float32)
    sum_squares, sum_products = packed_total(
        (jnp.sum(attended * attended, axis=-1), jnp.sum(attended * scaled, axis=-1)), "tp"
    )
    full_width = width_dev * lax.axis_size("tp")
    inv_rms = lax.rsqrt(sum_squares / full_width + epsilon)[..., None]
    mean_prod = (sum_products / full_width)[..., None]
    grad_attended = (inv_rms * scaled - attended * inv_rms**3 * mean_prod).astype(jnp.bfloat16)
    grad_seg = as_segments(grad_attended)
    grad_probs = band_products(grad_seg, value_all, seg_count, band_len)
    row_dot = jnp.sum(probability * grad_probs, axis=-1, keepdims=True)
    grad_scores = probability * (grad_probs - row_dot)
    grad_low = grad_scores.astype(jnp.bfloat16)
    grad_table = one_axis_at_a_time(pullback(jnp.sum(grad_scores, axis=(0, 2)))[0], SP)
    grad_query = sum(
        (
            jnp.einsum(
                "bhcqk,bckhd->bcqhd",
                band_slice(grad_low, offset),
                key_all[:, offset : offset + seg_count],
                preferred_element_type=jnp.float32,
            )
            for offset in range(band_len)
        )
    )
    key_pad = place(
        [(offset, key_terms(grad_low, query_seg, offset)) for offset in range(band_len)],
        seg_count + LEFT,
    )
    value_pad = place(
        [(offset, key_terms(prob_low, grad_seg, offset)) for offset in range(band_len)],
        seg_count + LEFT,
    )
    back_keys, back_values = passed_along((key_pad[:, :LEFT], value_pad[:, :LEFT]), SP, -1)
    key_grad = at_tail(key_pad[:, LEFT:], back_keys)
    value_grad = at_tail(value_pad[:, LEFT:], back_values)
    grad_queries = (grad_query.reshape(seq_count, row_count, width_dev) / scale_root).astype(
        jnp.bfloat16
    )
    grad_keys = (key_grad.reshape(seq_count, row_count, width_dev) / scale_root).astype(
        jnp.bfloat16
    )
    grad_values = value_grad.reshape(seq_count, row_count, width_dev).astype(jnp.bfloat16)
    return (grad_queries, grad_keys, grad_values, grad_table)


def solution(mesh):
    finer = Mesh(mesh.devices.reshape(12, 8, mesh.shape["tp"]), ("sp_0", "sp_1", "tp"))
    placed = (
        P(None, SP, "tp"),
        P(None, SP, "tp"),
        P(None, SP, "tp"),
        P(None, SP, "tp"),
        P("tp"),
        P("tp", None),
    )
    return jax.shard_map(
        on_device,
        mesh=finer,
        in_specs=placed,
        out_specs=(P(None, SP, "tp"), P(None, SP, "tp"), P(None, SP, "tp"), P("tp", None)),
        check_vma=False,
    )
```

profile of v0, /device:TPU:2, one launch (start us, length us, event | category | flops | bytes accessed | tf_op | source)
XLA Modules:
  0.0 131.9 jit_solution(16314634308907737492)
XLA Ops:
  0.6 3.5 %collective-permute-start = (bf16[1,256,256]{2,1,0:T(8,128)(2,1)}, bf16[1,256,256]{2,1,0:T(8,128)(2,1)S(1)}, u32[]{:S(2)}, u32[]{:S(2)}) collective-permute-start(bf16[1,256,256]{2,1,0:T(8,128)(2,1)} %param.7), channel_id=1, source_target_pairs={{0,8},{8,16},{16,24},{24,32},{32,40},{40,48},{48,56},{56,64},{64,7... | collective-permute-start | bytes 393224 | tf_op jit(solution)/shard_map/ppermute | solution.py:23
  4.1 3.5 %collective-permute-start.1 = (bf16[1,256,256]{2,1,0:T(8,128)(2,1)}, bf16[1,256,256]{2,1,0:T(8,128)(2,1)S(1)}, u32[]{:S(2)}, u32[]{:S(2)}) collective-permute-start(bf16[1,256,256]{2,1,0:T(8,128)(2,1)} %param.8), channel_id=1, source_target_pairs={{0,8},{8,16},{16,24},{24,32},{32,40},{40,48},{48,56},{56,64},{64,7... | collective-permute-start | bytes 393224 | tf_op jit(solution)/shard_map/ppermute | solution.py:23
  7.6 0.7 convert_element_type.91
  13.8 0.7 reverse.64
  14.7 0.9 copy-done.2
  15.9 0.6 copy-done.6
  16.6 0.5 fusion.201
  19.5 0.7 copy-done.4
  22.1 0.6 copy-done.1
  22.8 11.4 %all_to_all.6 = f32[8,1,512]{2,1,0:T(1,128)S(1)} all-to-all(f32[8,1,512]{2,1,0:T(1,128)S(1)} %broadcast_in_dim.45), channel_id=1, replica_groups=mesh['sp_0'=12,'sp_1'=8,'tp'=8] {'tp'}, dimensions={0} | all-to-all | bytes 32768 | tf_op jit(solution)/shard_map/all_to_all | solution.py:28
  34.3 0.8 subtract_convert_fusion
  35.1 0.9 reshape.784
  36.0 0.9 convolution_bitcast_fusion.10
  37.0 0.9 convolution_bitcast_fusion.11
  37.9 0.9 convolution_bitcast_fusion.12
  38.8 0.9 convolution_bitcast_fusion.13
  39.7 0.9 convolution_bitcast_fusion.14
  40.6 1.5 %concatenate.101 = f32[1,2,4,64,320]{4,3,2,1,0:T(8,128)S(1)} concatenate(f32[1,2,4,64,64]{4,3,2,1,0:T(8,128)} %convolution_bitcast_fusion.14, f32[1,2,4,64,64]{4,3,2,1,0:T(8,128)} %convolution_bitcast_fusion.13, f32[1,2,4,64,64]{4,3,2,1,0:T(8,128)} %convolution_bitcast_fusion.12, f32[1,2,4,64,64]{4,3,2,1,0:T(8,128)} %convolution_bitcast_fusion.11, ...), dimensions={4} | concatenate | bytes 1310720 | tf_op jit(solution)/shard_map/concatenate | solution.py:69
  43.8 0.9 convolution_bitcast_fusion.1
  44.7 0.9 convolution_bitcast_fusion
  45.8 0.9 convolution_bitcast_fusion.9
  69.8 1.1 pad_add_fusion
  71.0 1.3 collective-permute-start.3
  73.2 0.7 copy-done
  74.0 0.7 slice.590
  74.7 1.3 collective-permute-start.2
  76.9 0.7 convert_element_type.98
  77.7 34.6 %psum.14 = f32[2,320]{1,0:T(2,128)S(1)} all-reduce(f32[2,320]{1,0:T(2,128)S(1)} %slice_add_fusion.2), channel_id=1, replica_groups=mesh['sp_0'=12,'sp_1'=8,'tp'=8] {'sp_0'}, use_global_device_ids=true, to_apply=%region_8.9 | all-reduce | flops 640 | bytes 5120 | tf_op jit(solution)/shard_map/psum | solution.py:47
  112.3 16.8 %psum.15 = f32[2,320]{1,0:T(2,128)} all-reduce(f32[2,320]{1,0:T(2,128)S(1)} %psum.14), channel_id=1, replica_groups=mesh['sp_0'=12,'sp_1'=8,'tp'=8] {'sp_1'}, use_global_device_ids=true, to_apply=%region_9.10 | all-reduce | flops 640 | bytes 5120 | tf_op jit(solution)/shard_map/psum | solution.py:47
  129.2 0.7 convert_element_type.102
  130.0 1.0 fusion.11
  131.1 0.7 convert_element_type.100
  (335 shorter events, 37.3 us)
Async XLA Ops:
  0.6 7.7 %copy-start.5 = (bf16[2,320]{1,0:T(2,128)(2,1)S(1)}, bf16[2,320]{1,0:T(2,128)(2,1)}, u32[]{:S(2)}) copy-start(bf16[2,320]{1,0:T(2,128)(2,1)} %param.11) | copy-start | bytes 3844
  0.6 15.9 %collective-permute-start = (bf16[1,256,256]{2,1,0:T(8,128)(2,1)}, bf16[1,256,256]{2,1,0:T(8,128)(2,1)S(1)}, u32[]{:S(2)}, u32[]{:S(2)}) collective-permute-start(bf16[1,256,256]{2,1,0:T(8,128)(2,1)} %param.7), channel_id=1, source_target_pairs={{0,8},{8,16},{16,24},{24,32},{32,40},{40,48},{48,56},{56,64},{64,7... | collective-permute-start | bytes 393224 | tf_op jit(solution)/shard_map/ppermute | solution.py:23
  4.1 15.3 %collective-permute-start.1 = (bf16[1,256,256]{2,1,0:T(8,128)(2,1)}, bf16[1,256,256]{2,1,0:T(8,128)(2,1)S(1)}, u32[]{:S(2)}, u32[]{:S(2)}) collective-permute-start(bf16[1,256,256]{2,1,0:T(8,128)(2,1)} %param.8), channel_id=1, source_target_pairs={{0,8},{8,16},{16,24},{24,32},{32,40},{40,48},{48,56},{56,64},{64,7... | collective-permute-start | bytes 393224 | tf_op jit(solution)/shard_map/ppermute | solution.py:23
  14.7 0.9 copy-start.2
  15.6 0.9 copy-start.3
  15.8 0.7 copy-start.6
  19.3 0.9 copy-start.4
  21.8 0.9 copy-start.1
  71.0 58.1 %collective-permute-start.3 = (f32[1,4,64,2,128]{4,2,3,1,0:T(8,128)S(1)}, f32[1,4,64,2,128]{4,2,3,1,0:T(8,128)S(1)}, u32[]{:S(2)}, u32[]{:S(2)}) collective-permute-start(f32[1,4,64,2,128]{4,2,3,1,0:T(8,128)S(1)} %slice.592), channel_id=1, source_target_pairs={{8,0},{16,8},{24,16},{32,24},{40,32},{48,40},{56,48},{64,56},{72,6... | collective-permute-start | bytes 786440 | tf_op jit(solution)/shard_map/ppermute | solution.py:23
  73.0 1.0 copy-start
  74.7 55.3 %collective-permute-start.2 = (f32[1,4,64,2,128]{4,2,3,1,0:T(8,128)}, f32[1,4,64,2,128]{4,2,3,1,0:T(8,128)}, u32[]{:S(2)}, u32[]{:S(2)}) collective-permute-start(f32[1,4,64,2,128]{4,2,3,1,0:T(8,128)} %slice.590), channel_id=1, source_target_pairs={{8,0},{16,8},{24,16},{32,24},{40,32},{48,40},{56,48},{64,56},{72,6... | collective-permute-start | bytes 786440 | tf_op jit(solution)/shard_map/ppermute | solution.py:23
where the time goes:
time: 132 us
  blocking collectives  62.8 us (48%)
  local copies, waits for them, and re-layouts  35.4 us (27%)
  matrix products  11.6 us (9%)
  other arithmetic  11.2 us (8%)
  starting transfers between devices  9.55 us (7%)
    psum x2, blocking collectives, one_axis_at_a_time(): x = lax.psum(x, axis)  51.4 us
    unnamed x145, local copies, waits for them, and re-layouts  21.9 us
    all_to_all x1, blocking collectives, sent_to_all(): return lax.all_to_all(copies, axis, split_axis=0, concat_axis=0, tiled=True)  11.4 us
    ppermute x4, starting transfers between devices, passed_along(): return lax.ppermute(block, axis, route)  9.55 us
    dot_general x10, matrix products, band_products(): jnp.einsum('bcqhd,bckhd->bhcqk', left_seg, right_all[:, offset:offset + s...  5.51 us
    unnamed x63, other arithmetic  5.09 us
    another operation x67, local copies, waits for them, and re-layouts, flat_bias(): jnp.stack([extended[:, offset:offset + band_width] for offset in range(SE...  4.89 us
    dot_general x10, matrix products, key_terms(): jnp.einsum('bhcqk,bcqhd->bckhd', band_slice(weights, offset), rows_seg, p...  4.38 us
  transfers between devices with their start and end apart: 4, of which 0 were waited for; matrix products, arithmetic and copies ran while one was open for 11% of the time, Pallas kernels for 0%

commit v1 on v0

v1 whole, which is shorter than its diff:
```python
import functools
import math

import jax
import jax.numpy as jnp
from jax import lax
from jax.experimental import pallas as pl
from jax.experimental.pallas import tpu as pltpu
from jax.sharding import Mesh
from jax.sharding import PartitionSpec as P

HEAD_DIM = 128
SEG = 64
LEFT = 4
MAX_REL = 256
REL = 320
SP = ("sp_0", "sp_1")

PAIR = 2 * SEG
WINDOW = (LEFT + 2) * SEG
epsilon = 1e-06
masked_value = -1e30
f32 = jnp.float32
bf16 = jnp.bfloat16
exact = lax.Precision.HIGHEST
VMEM = pl.BlockSpec(memory_space=pltpu.VMEM)
SMEM = pl.BlockSpec(memory_space=pltpu.SMEM)


def dot(left, right, dims, precision=None):
    return lax.dot_general(
        left, right, (dims, ((), ())), preferred_element_type=f32, precision=precision
    )


def passed_along(block, axis, distance):
    devices = range(lax.axis_size(axis))
    route = [(i - distance, i) for i in devices if i - distance in devices]
    return lax.ppermute(block, axis, route)


def sent_to_all(copies, axis):
    return lax.all_to_all(copies, axis, split_axis=0, concat_axis=0, tiled=True)


def mirror(rows, cols):
    row_id = lax.broadcasted_iota(jnp.int32, (rows, cols), 0)
    col_id = lax.broadcasted_iota(jnp.int32, (rows, cols), 1)
    return row_id + col_id == REL - 1


def diagonal_sums(block):
    width = block.shape[1]
    folded = block[:8]
    for at in range(8, block.shape[0], 8):
        folded = folded + pltpu.roll(block[at : at + 8], width - at, 1)
    row = lax.broadcasted_iota(jnp.int32, folded.shape, 0)
    for step in (1, 2, 4):
        folded = jnp.where((row & step) != 0, pltpu.roll(folded, width - step, 1), folded)
    return jnp.sum(folded, axis=0, keepdims=True)


def bias_kernel(first_ref, rel_ref, bias_ref):
    heads, pairs = bias_ref.shape[:2]
    turned = dot(rel_ref[...], mirror(REL, WINDOW).astype(bf16), ((1,), (0,)))
    row = lax.broadcasted_iota(jnp.int32, (PAIR, WINDOW), 0)
    col = lax.broadcasted_iota(jnp.int32, (PAIR, WINDOW), 1)
    base = jnp.where(row >= SEG, SEG, 0)
    in_band = (col >= base) & (col < base + (LEFT + 1) * SEG)
    first = first_ref[0] == 1
    for h in range(heads):
        line = turned[h : h + 1]
        slid = pltpu.roll(jnp.broadcast_to(line, (PAIR, WINDOW)), 0, 1, stride=1, stride_axis=0)
        tile = jnp.where(col < row, jnp.broadcast_to(line[:, :1], (PAIR, WINDOW)), slid)
        tile = jnp.where(in_band, tile, masked_value)
        for g in range(pairs):
            start = jnp.where(first, LEFT * SEG - g * PAIR, 0)
            bias_ref[h, g] = jnp.where(col >= start, tile, masked_value)


def forward_kernel(
    q_ref, k_ref, v_ref, prior_ref, bias_ref, cot_ref, gain_ref, prob_ref, att_ref, stat_ref
):
    rows, width = q_ref.shape
    heads, pairs = width // HEAD_DIM, rows // PAIR
    scale_root = math.sqrt(HEAD_DIM)
    totals = None
    products = None
    ones = jnp.ones((8, HEAD_DIM), f32)
    for h in range(heads):
        ch = slice(h * HEAD_DIM, (h + 1) * HEAD_DIM)
        keys = jnp.concatenate([prior_ref[:rows, ch], k_ref[:, ch]], axis=0)
        values = jnp.concatenate([prior_ref[rows:, ch], v_ref[:, ch]], axis=0)
        outs = []
        for g in range(pairs):
            band = slice(g * PAIR, g * PAIR + WINDOW)
            here = slice(g * PAIR, (g + 1) * PAIR)
            scores = dot(q_ref[here, ch], keys[band], ((1,), (1,))) / scale_root + bias_ref[h, g]
            top = jnp.max(scores, axis=-1, keepdims=True)
            shifted = jnp.exp(scores - top)
            prob = shifted / jnp.sum(shifted, axis=-1, keepdims=True)
            prob_ref[h, g] = prob
            out = dot(prob.astype(bf16), values[band], ((1,), (0,)))
            att_ref[here, ch] = out
            outs.append(out)
        out = jnp.concatenate(outs, axis=0)
        scaled = cot_ref[:, ch].astype(f32) * gain_ref[:, ch].astype(f32)
        square = dot(ones, out * out, ((1,), (1,)), exact)
        product = dot(ones, out * scaled, ((1,), (1,)), exact)
        totals = square if totals is None else totals + square
        products = product if products is None else products + product
    half = rows // 2
    message = jnp.concatenate(
        [totals[:1, :half], totals[:1, half:], products[:1, :half], products[:1, half:]], axis=0
    )
    for d in range(stat_ref.shape[0]):
        stat_ref[d] = message


def backward_kernel(
    q_ref,
    k_ref,
    v_ref,
    prior_ref,
    cot_ref,
    gain_ref,
    prob_ref,
    att_ref,
    stat_ref,
    dq_ref,
    dk_ref,
    dv_ref,
    back_ref,
    table_ref,
    *,
    full_width,
):
    rows, width = q_ref.shape
    heads, pairs = width // HEAD_DIM, rows // PAIR
    half = rows // 2
    scale_root = math.sqrt(HEAD_DIM)
    summed = stat_ref[0]
    for d in range(1, stat_ref.shape[0]):
        summed = summed + stat_ref[d]
    pick = lax.broadcasted_iota(jnp.int32, (4, 4 * HEAD_DIM), 1) // HEAD_DIM
    pick = (pick == lax.broadcasted_iota(jnp.int32, (4, 4 * HEAD_DIM), 0)).astype(f32)
    spread = dot(summed, pick, ((0,), (0,)), exact)
    squares = jnp.concatenate([spread[:, :128], spread[:, 128:256]], axis=0)
    products = jnp.concatenate([spread[:, 256:384], spread[:, 384:]], axis=0)
    inv_rms = lax.rsqrt(squares / full_width + epsilon)
    pull = inv_rms**3 * (products / full_width)
    lines = []
    for h in range(heads):
        ch = slice(h * HEAD_DIM, (h + 1) * HEAD_DIM)
        keys = jnp.concatenate([prior_ref[:rows, ch], k_ref[:, ch]], axis=0)
        values = jnp.concatenate([prior_ref[rows:, ch], v_ref[:, ch]], axis=0)
        scaled = cot_ref[:, ch].astype(f32) * gain_ref[:, ch].astype(f32)
        grad = (inv_rms * scaled - att_ref[:, ch] * pull).astype(bf16)
        summed_scores = None
        key_parts = []
        value_parts = []
        for g in range(pairs):
            band = slice(g * PAIR, g * PAIR + WINDOW)
            here = slice(g * PAIR, (g + 1) * PAIR)
            prob = prob_ref[h, g]
            grad_probs = dot(grad[here], values[band], ((1,), (1,)))
            row_dot = jnp.sum(prob * grad_probs, axis=-1, keepdims=True)
            grad_scores = prob * (grad_probs - row_dot)
            grad_low = grad_scores.astype(bf16)
            summed_scores = grad_scores if summed_scores is None else summed_scores + grad_scores
            dq = dot(grad_low, keys[band], ((1,), (0,))) / scale_root
            dq_ref[here, ch] = dq.astype(bf16)
            key_parts.append(dot(grad_low, q_ref[here, ch], ((0,), (0,))))
            value_parts.append(dot(prob.astype(bf16), grad[here], ((0,), (0,))))
        lower = pltpu.roll(summed_scores[SEG:], WINDOW - SEG, 1)
        joined = summed_scores[:SEG] + lower
        lines.append(diagonal_sums(joined))
        for parts, back_at, own_ref, scale in (
            (key_parts, 0, dk_ref, scale_root),
            (value_parts, rows, dv_ref, 1.0),
        ):
            merged = []
            for block in range((rows + LEFT * SEG) // PAIR):
                total = None
                for g in range(pairs):
                    at = block - g
                    if 0 <= at < WINDOW // PAIR:
                        part = parts[g][at * PAIR : (at + 1) * PAIR]
                        total = part if total is None else total + part
                merged.append(total)
            merged = jnp.concatenate(merged, axis=0) / scale
            back_ref[back_at : back_at + rows, ch] = merged[: LEFT * SEG].astype(bf16)
            own_ref[:, ch] = merged[LEFT * SEG :]
    line = jnp.concatenate(lines, axis=0)
    col = lax.broadcasted_iota(jnp.int32, line.shape, 1)
    wrapped = jnp.sum(jnp.where(col > REL, line, 0.0), axis=1, keepdims=True)
    line = jnp.where(col == 0, line + wrapped, line)
    for h in range(heads):
        table_ref[:, :, h * REL : (h + 1) * REL] = jnp.broadcast_to(
            line[h : h + 1, :REL][None], (table_ref.shape[0], 1, REL)
        )


def final_kernel(dk_ref, dv_ref, back_ref, key_ref, value_ref):
    rows = dk_ref.shape[0]
    key_ref[...] = (dk_ref[...] + back_ref[:rows].astype(f32)).astype(bf16)
    value_ref[...] = (dv_ref[...] + back_ref[rows:].astype(f32)).astype(bf16)


def table_kernel(all_ref, table_ref):
    heads = table_ref.shape[0]
    total = jnp.sum(all_ref[...], axis=0)
    lines = jnp.concatenate([total[:, h * REL : (h + 1) * REL] for h in range(heads)], axis=0)
    table_ref[...] = dot(lines, mirror(REL, REL).astype(f32), ((1,), (0,)), exact)


def call(kernel, outs, in_specs=None, n_in=0):
    return pl.pallas_call(
        kernel,
        out_shape=outs,
        in_specs=in_specs or [VMEM] * n_in,
        out_specs=jax.tree.map(lambda _: VMEM, outs),
    )


def on_device(queries, key_vectors, value_vectors, cotangent, out_gain, rel_table):
    shape = queries.shape
    rows, width = shape[1], shape[2]
    heads, pairs = width // HEAD_DIM, rows // PAIR
    q, k, v, cot = (a.reshape(rows, width) for a in (queries, key_vectors, value_vectors, cotangent))
    gain = out_gain.reshape(1, width)
    members = lax.axis_size("tp")
    out = jax.ShapeDtypeStruct
    prior = passed_along(jnp.concatenate([k, v], axis=0), SP, 1)
    first = (lax.axis_index(SP) == 0).astype(jnp.int32).reshape(1)
    bias = call(bias_kernel, out((heads, pairs, PAIR, WINDOW), f32), [SMEM, VMEM])(first, rel_table)
    prob, att, stat = call(
        forward_kernel,
        (
            out((heads, pairs, PAIR, WINDOW), f32),
            out((rows, width), f32),
            out((members, 4, rows // 2), f32),
        ),
        n_in=7,
    )(q, k, v, prior, bias, cot, gain)
    stat = sent_to_all(stat, "tp")
    dq, dk, dv, back, table = call(
        functools.partial(backward_kernel, full_width=width * members),
        (
            out((rows, width), bf16),
            out((rows, width), f32),
            out((rows, width), f32),
            out((2 * rows, width), bf16),
            out((lax.axis_size(SP), 1, heads * REL), f32),
        ),
        n_in=9,
    )(q, k, v, prior, cot, gain, prob, att, stat)
    back = passed_along(back, SP, -1)
    table = sent_to_all(table, SP)
    grad_keys, grad_values = call(
        final_kernel, (out((rows, width), bf16), out((rows, width), bf16)), n_in=3
    )(dk, dv, back)
    grad_table = call(table_kernel, out((heads, REL), f32), n_in=1)(table)
    return (dq.reshape(shape), grad_keys.reshape(shape), grad_values.reshape(shape), grad_table)


def solution(mesh):
    finer = Mesh(mesh.devices.reshape(12, 8, mesh.shape["tp"]), ("sp_0", "sp_1", "tp"))
    placed = (
        P(None, SP, "tp"),
        P(None, SP, "tp"),
        P(None, SP, "tp"),
        P(None, SP, "tp"),
        P("tp"),
        P("tp", None),
    )
    return jax.shard_map(
        on_device,
        mesh=finer,
        in_specs=placed,
        out_specs=(P(None, SP, "tp"), P(None, SP, "tp"), P(None, SP, "tp"), P("tp", None)),
        check_vma=False,
    )
```

time: 132 us -> 75.6 us (0.57)
  blocking collectives: 62.8 us -> 13.4 us
  local copies, waits for them, and re-layouts: 35.4 us -> 3.33 us
  waiting for transfers between devices: 0.01 us -> 17.8 us
  starting transfers between devices: 9.55 us -> 24.4 us
  Pallas kernels: 0 us -> 14.4 us
  matrix products: 11.6 us -> 0 us
  other arithmetic: 11.2 us -> 0.99 us
    psum x2 -> x0, blocking collectives: 51.4 us -> none  [one_axis_at_a_time(): x = lax.psum(x, axis)]
    all_to_all x0 -> x1, starting transfers between devices: none -> 19.6 us  [sent_to_all(): return lax.all_to_all(copies, axis, split_axis=0, concat_axis=0, tiled=True)]
    unnamed x145 -> x10, local copies, waits for them, and re-layouts: 21.9 us -> 2.77 us
    ppermute x4 -> x2, waiting for transfers between devices: 0.01 us -> 15 us  [passed_along(): return lax.ppermute(block, axis, route)]
    pallas_call x0 -> x5, Pallas kernels: none -> 14.4 us  [the longest x1 4.58 us: on_device(): call(functools.partial(backward_kernel, full_width=width * members), (out...]
    dot_general x30 -> x0, matrix products: 11.6 us -> none  [the longest x10 5.51 us: band_products(): jnp.einsum('bcqhd,bckhd->bhcqk', left_seg, right_all[:, offset:offset + s...]
    another operation x71 -> x0, local copies, waits for them, and re-layouts: 6.22 us -> none  [the longest x67 4.89 us: flat_bias(): jnp.stack([extended[:, offset:offset + band_width] for offset in range(SE...]
    unnamed x63 -> x0, other arithmetic: 5.09 us -> none
  transfers between devices with their start and end apart: 4 -> 3, of which waited for: 0 -> 3; matrix products, arithmetic and copies ran while one was open for 11% -> 1% of each run, Pallas kernels for 0% -> 5%
where the time goes in v1:
time: 75.6 us; the launch traced here: 75.1 us
  starting transfers between devices  24.4 us (32%)
  waiting for transfers between devices  17.8 us (24%)
  Pallas kernels  14.4 us (19%)
  blocking collectives  13.4 us (18%)
  local copies, waits for them, and re-layouts  3.33 us (4%)
  other arithmetic  0.99 us (1%)
    all_to_all x1, starting transfers between devices, sent_to_all(): return lax.all_to_all(copies, axis, split_axis=0, concat_axis=0, tiled=True)  19.6 us
    ppermute x2, waiting for transfers between devices, passed_along(): return lax.ppermute(block, axis, route)  15 us
    all_to_all x1, blocking collectives, sent_to_all(): return lax.all_to_all(copies, axis, split_axis=0, concat_axis=0, tiled=True)  13.4 us
    ppermute x2, starting transfers between devices, passed_along(): return lax.ppermute(block, axis, route)  4.79 us
    pallas_call x1, Pallas kernels, on_device(): call(functools.partial(backward_kernel, full_width=width * members), (out...  4.58 us
    pallas_call x1, Pallas kernels, on_device(): call(forward_kernel, (out((heads, pairs, PAIR, WINDOW), f32), out((rows,...  4.04 us
    all_to_all x1, waiting for transfers between devices, sent_to_all(): return lax.all_to_all(copies, axis, split_axis=0, concat_axis=0, tiled=True)  2.87 us
    unnamed x10, local copies, waits for them, and re-layouts  2.77 us
  transfers between devices with their start and end apart: 3, of which 3 were waited for; matrix products, arithmetic and copies ran while one was open for 1% of the time, Pallas kernels for 5%

profile of v1, /device:TPU:2, one launch (start us, length us, event | category | flops | bytes accessed | tf_op | source)
XLA Modules:
  0.0 75.1 jit_solution(631275268314801867)
XLA Ops:
  0.6 1.0 %pad_maximum_fusion = bf16[512,256]{1,0:T(8,128)(2,1)S(1)} fusion(bf16[256,256]{1,0:T(8,128)(2,1)} %bitcast.11, bf16[256,256]{1,0:T(8,128)(2,1)} %bitcast.8), kind=kLoop, calls=%fused_computation | loop fusion | flops 524288 | bytes 524288 | tf_op jit(solution)/shard_map/concatenate | solution.py:234
  1.6 3.5 %collective-permute-start = (bf16[512,256]{1,0:T(8,128)(2,1)S(1)}, bf16[512,256]{1,0:T(8,128)(2,1)S(1)}, u32[]{:S(2)}, u32[]{:S(2)}) collective-permute-start(bf16[512,256]{1,0:T(8,128)(2,1)S(1)} %pad_maximum_fusion), channel_id=1, source_target_pairs={{0,8},{8,16},{16,24},{24,32},{32,40},{40,48},{48,56},{56,64},{64,7... | collective-permute-start | bytes 786440 | tf_op jit(solution)/shard_map/ppermute | solution.py:39
  5.1 0.0 copy-start.4
  5.2 0.6 copy-done.4
  5.8 0.6 reshape.41.gain_ref
  6.4 1.9 %shard_map.93.bias_ref = f32[2,2,128,384]{3,2,1,0:T(8,128)} custom-call(s32[1]{0:T(128)} %bitcast.4.first_ref, bf16[2,320]{1,0:T(2,128)(2,1)} %rel_ref.1), custom_call_target="tpu_custom_call" | custom-call | tf_op jit(solution)/shard_map/pallas_call | solution.py:236
  8.3 2.4 %collective-permute-done.prior_ref = bf16[512,256]{1,0:T(8,128)(2,1)S(1)} collective-permute-done((bf16[512,256]{1,0:T(8,128)(2,1)S(1)}, bf16[512,256]{1,0:T(8,128)(2,1)S(1)}, u32[]{:S(2)}, u32[]{:S(2)}) %collective-permute-start) | collective-permute-done | bytes 262176 | tf_op jit(solution)/shard_map/ppermute | solution.py:39
  10.7 0.0 copy-start
  10.7 0.7 copy-done
  11.4 4.0 %shard_map.94 = (f32[2,2,128,384]{3,2,1,0:T(8,128)}, f32[256,256]{1,0:T(8,128)}, f32[8,4,128]{2,1,0:T(4,128)}) custom-call(bf16[256,256]{1,0:T(8,128)(2,1)} %bitcast.14, bf16[256,256]{1,0:T(8,128)(2,1)} %bitcast.9, bf16[256,256]{1,0:T(8,128)(2,1)} %bitcast.12, bf16[512,256]{1,0:T(8,128)(2,1)} %copy-done, f32[2,2,128,384]{3,2,1,0:T(8,128)} %shard_map.93.bias_ref, ...), custom_call_target="tpu_custom_call" | custom-call | tf_op jit(solution)/shard_map/pallas_call | solution.py:237
  15.4 13.4 %all_to_all.10.stat_ref = f32[8,4,128]{2,1,0:T(4,128)} all-to-all(f32[8,4,128]{2,1,0:T(4,128)} %get-tuple-element.16), channel_id=1, replica_groups=mesh['sp_0'=12,'sp_1'=8,'tp'=8] {'tp'}, dimensions={0} | all-to-all | bytes 32768 | tf_op jit(solution)/shard_map/all_to_all | solution.py:43
  28.8 4.6 %shard_map.95 = (bf16[256,256]{1,0:T(8,128)(2,1)}, f32[256,256]{1,0:T(8,128)}, f32[256,256]{1,0:T(8,128)}, bf16[512,256]{1,0:T(8,128)(2,1)}, f32[96,1,640]{2,1,0:T(1,128)}) custom-call(bf16[256,256]{1,0:T(8,128)(2,1)} %bitcast.15, bf16[256,256]{1,0:T(8,128)(2,1)} %bitcast.10, bf16[256,256]{1,0:T(8,128)(2,1)} %bitcast.13, bf16[512,256]{1,0:T(8,128)(2,1)} %copy-done, ...), custom_call_target="tpu_custom_call" | custom-call | tf_op jit(solution)/shard_map/pallas_call | solution.py:247
  33.4 0.0 copy-start.3
  33.4 19.6 %all-to-all-start.1 = ((f32[96,1,640]{2,1,0:T(1,128)}), f32[96,1,640]{2,1,0:T(1,128)S(1)}, u32[]{:S(2)}, u32[]{:S(2)}) async-start(f32[96,1,640]{2,1,0:T(1,128)} %get-tuple-element.23), calls=%async_computation.1 | async-start | bytes 491520 | tf_op jit(solution)/shard_map/all_to_all | solution.py:43
  53.1 0.0 copy-done.3
  53.1 1.3 %collective-permute-start.1 = (bf16[512,256]{1,0:T(8,128)(2,1)S(1)}, bf16[512,256]{1,0:T(8,128)(2,1)S(1)}, u32[]{:S(2)}, u32[]{:S(2)}) collective-permute-start(bf16[512,256]{1,0:T(8,128)(2,1)S(1)} %copy-done.3), channel_id=1, source_target_pairs={{8,0},{16,8},{24,16},{32,24},{40,32},{48,40},{56,48},{64,56},{72,6... | collective-permute-start | bytes 786440 | tf_op jit(solution)/shard_map/ppermute | solution.py:39
  54.4 12.6 %collective-permute-done.1.back_ref = bf16[512,256]{1,0:T(8,128)(2,1)S(1)} collective-permute-done((bf16[512,256]{1,0:T(8,128)(2,1)S(1)}, bf16[512,256]{1,0:T(8,128)(2,1)S(1)}, u32[]{:S(2)}, u32[]{:S(2)}) %collective-permute-start.1) | collective-permute-done | bytes 262176 | tf_op jit(solution)/shard_map/ppermute | solution.py:39
  67.0 0.0 copy-start.2
  67.0 0.7 copy-done.2
  67.7 1.8 %shard_map.96 = (bf16[256,256]{1,0:T(8,128)(2,1)}, bf16[256,256]{1,0:T(8,128)(2,1)}) custom-call(f32[256,256]{1,0:T(8,128)} %get-tuple-element.18.dk_ref, f32[256,256]{1,0:T(8,128)} %get-tuple-element.19.dv_ref, bf16[512,256]{1,0:T(8,128)(2,1)} %copy-done.2), custom_call_target="tpu_custom_call" | custom-call | tf_op jit(solution)/shard_map/pallas_call | solution.py:260
  69.5 2.9 %all-to-all-done.1.all_ref = f32[96,1,640]{2,1,0:T(1,128)S(1)} async-done(((f32[96,1,640]{2,1,0:T(1,128)}), f32[96,1,640]{2,1,0:T(1,128)S(1)}, u32[]{:S(2)}, u32[]{:S(2)}) %all-to-all-start.1) | async-done | bytes 245792 | tf_op jit(solution)/shard_map/all_to_all | solution.py:43
  72.4 0.0 copy-start.1
  72.4 0.7 copy-done.1
  73.1 2.0 %shard_map.97 = f32[2,320]{1,0:T(2,128)} custom-call(f32[96,1,640]{2,1,0:T(1,128)} %copy-done.1), custom_call_target="tpu_custom_call" | custom-call | tf_op jit(solution)/shard_map/pallas_call | solution.py:263
Async XLA Ops:
  1.6 9.0 %collective-permute-start = (bf16[512,256]{1,0:T(8,128)(2,1)S(1)}, bf16[512,256]{1,0:T(8,128)(2,1)S(1)}, u32[]{:S(2)}, u32[]{:S(2)}) collective-permute-start(bf16[512,256]{1,0:T(8,128)(2,1)S(1)} %pad_maximum_fusion), channel_id=1, source_target_pairs={{0,8},{8,16},{16,24},{24,32},{32,40},{40,48},{48,56},{56,64},{64,7... | collective-permute-start | bytes 786440 | tf_op jit(solution)/shard_map/ppermute | solution.py:39
  5.1 0.7 copy-start.4
  10.7 0.7 copy-start
  33.4 19.7 %copy-start.3 = (bf16[512,256]{1,0:T(8,128)(2,1)S(1)}, bf16[512,256]{1,0:T(8,128)(2,1)}, u32[]{:S(2)}) copy-start(bf16[512,256]{1,0:T(8,128)(2,1)} %get-tuple-element.20) | copy-start | bytes 786436
  33.4 38.9 %all-to-all-start.1 = ((f32[96,1,640]{2,1,0:T(1,128)}), f32[96,1,640]{2,1,0:T(1,128)S(1)}, u32[]{:S(2)}, u32[]{:S(2)}) async-start(f32[96,1,640]{2,1,0:T(1,128)} %get-tuple-element.23), calls=%async_computation.1 | async-start | bytes 491520 | tf_op jit(solution)/shard_map/all_to_all | solution.py:43
  53.1 13.9 %collective-permute-start.1 = (bf16[512,256]{1,0:T(8,128)(2,1)S(1)}, bf16[512,256]{1,0:T(8,128)(2,1)S(1)}, u32[]{:S(2)}, u32[]{:S(2)}) collective-permute-start(bf16[512,256]{1,0:T(8,128)(2,1)S(1)} %copy-done.3), channel_id=1, source_target_pairs={{8,0},{16,8},{24,16},{32,24},{40,32},{48,40},{56,48},{64,56},{72,6... | collective-permute-start | bytes 786440 | tf_op jit(solution)/shard_map/ppermute | solution.py:39
  67.0 0.7 copy-start.2
  72.4 0.7 copy-start.1

commit v2 on v1

v2 whole, which is shorter than its diff:
```python
import functools
import math

import jax
import jax.numpy as jnp
from jax import lax
from jax.experimental import pallas as pl
from jax.experimental.pallas import tpu as pltpu
from jax.sharding import Mesh
from jax.sharding import PartitionSpec as P


HEAD_DIM = 128
SEG = 64
LEFT = 4
REL = 320
SP = ("sp_0", "sp_1")

PAIR = 2 * SEG
PRIOR = LEFT * SEG
WINDOW = PRIOR + PAIR
ROOM = 12 * 1024 * 1024
epsilon = 1e-06
masked_value = -1e30
f32 = jnp.float32
bf16 = jnp.bfloat16
exact = lax.Precision.HIGHEST
kept = pltpu.VMEM
out = jax.ShapeDtypeStruct
VMEM = pl.BlockSpec(memory_space=pltpu.VMEM)
HBM = pl.BlockSpec(memory_space=pltpu.HBM)
SMEM = pl.BlockSpec(memory_space=pltpu.SMEM)


def dot(left, right, dims, precision=None):
    return lax.dot_general(
        left, right, (dims, ((), ())), preferred_element_type=f32, precision=precision
    )


def parts_of(array, count):
    found = []
    for _ in range(count):
        found.append(array.astype(bf16))
        array = array - found[-1].astype(f32)
    return found


def passed_along(block, axis, distance):
    devices = range(lax.axis_size(axis))
    route = [(i - distance, i) for i in devices if i - distance in devices]
    return lax.ppermute(block, axis, route)


def sent_to_all(copies, axis):
    return lax.all_to_all(copies, axis, split_axis=0, concat_axis=0, tiled=True)


def mirror(rows, cols):
    row_id = lax.broadcasted_iota(jnp.int32, (rows, cols), 0)
    col_id = lax.broadcasted_iota(jnp.int32, (rows, cols), 1)
    return row_id + col_id == REL - 1


def diagonal_sums(block):
    width = block.shape[1]
    folded = block[:8]
    for at in range(8, block.shape[0], 8):
        folded = folded + pltpu.roll(block[at : at + 8], width - at, 1)
    row = lax.broadcasted_iota(jnp.int32, folded.shape, 0)
    for step in (1, 2, 4):
        folded = jnp.where((row & step) != 0, pltpu.roll(folded, width - step, 1), folded)
    return jnp.sum(folded, axis=0, keepdims=True)


def head_of(h):
    return slice(h * HEAD_DIM, (h + 1) * HEAD_DIM)


def rows_of(g):
    return slice(g * PAIR, (g + 1) * PAIR)


def early_kernel(
    first_ref,
    rel_ref,
    gain_ref,
    q_hbm,
    k_hbm,
    cot_hbm,
    v_hbm,
    q_ref,
    k_ref,
    v_ref,
    own_ref,
    bias_ref,
    scaled_ref,
    cot_ref,
    sems,
):
    rows, width = q_ref.shape
    heads, pairs = width // HEAD_DIM, rows // PAIR
    scale = 1.0 / math.sqrt(HEAD_DIM)
    moves = ((q_hbm, q_ref), (k_hbm, k_ref), (cot_hbm, cot_ref), (v_hbm, v_ref))
    copies = [pltpu.make_async_copy(a, b, sems.at[i]) for i, (a, b) in enumerate(moves)]
    for copy in copies:
        copy.start()
    turned = dot(rel_ref[...], mirror(REL, WINDOW).astype(bf16), ((1,), (0,)))
    row = lax.broadcasted_iota(jnp.int32, (PAIR, WINDOW), 0)
    col = lax.broadcasted_iota(jnp.int32, (PAIR, WINDOW), 1)
    base = jnp.where(row >= SEG, SEG, 0)
    in_band = (col >= base) & (col < base + PRIOR + SEG)
    first = first_ref[0] == 1
    for h in range(heads):
        line = turned[h : h + 1]
        slid = pltpu.roll(jnp.broadcast_to(line, (PAIR, WINDOW)), 0, 1, stride=1, stride_axis=0)
        tile = jnp.where(col < row, jnp.broadcast_to(line[:, :1], (PAIR, WINDOW)), slid)
        tile = jnp.where(in_band, tile, masked_value)
        for g in range(pairs):
            split = PRIOR - g * PAIR
            prior = tile[:, :split]
            bias_ref[h, g, :, :split] = jnp.where(first, masked_value, prior)
            own_ref[h, g, :, split:] = tile[:, split:]
    copies[0].wait()
    copies[1].wait()
    for h in range(heads):
        for g in range(pairs):
            split = PRIOR - g * PAIR
            own = dot(q_ref[rows_of(g), head_of(h)], k_ref[: (g + 1) * PAIR, head_of(h)], ((1,), (1,)))
            own_ref[h, g, :, split:] += own * scale
    copies[2].wait()
    scaled_ref[...] = cot_ref[...].astype(f32) * gain_ref[...].astype(f32)
    copies[3].wait()


def forward_kernel(
    q_ref, v_ref, prior_key_ref, prior_value_ref, own_ref, bias_ref, scaled_ref, prob_ref, att_ref, stat_ref
):
    rows, width = q_ref.shape
    heads, pairs = width // HEAD_DIM, rows // PAIR
    scale = 1.0 / math.sqrt(HEAD_DIM)
    squares = None
    products = None
    for h in range(heads):
        ch = head_of(h)
        outs = []
        for g in range(pairs):
            here = rows_of(g)
            split = PRIOR - g * PAIR
            scores = dot(q_ref[here, ch], prior_key_ref[g * PAIR : PRIOR, ch], ((1,), (1,)))
            scores = scores * scale + bias_ref[h, g, :, :split]
            scores = jnp.concatenate([scores, own_ref[h, g, :, split:]], axis=1)
            top = jnp.max(scores, axis=-1, keepdims=True)
            shifted = jnp.exp(scores - top)
            prob = shifted * (1.0 / jnp.sum(shifted, axis=-1, keepdims=True))
            prob_ref[h, g] = prob
            values = jnp.concatenate(
                [prior_value_ref[g * PAIR :, ch], v_ref[: (g + 1) * PAIR, ch]], axis=0
            )
            attended = dot(prob.astype(bf16), values, ((1,), (0,)))
            att_ref[here, ch] = attended
            outs.append(attended)
        attended = jnp.concatenate(outs, axis=0)
        square = attended * attended
        product = attended * scaled_ref[:, ch]
        squares = square if squares is None else squares + square
        products = product if products is None else products + product
    lines = []
    ones = jnp.ones((8, 2 * HEAD_DIM), bf16)
    for total in (squares, products):
        lines.append(dot(ones, jnp.concatenate(parts_of(total, 2), axis=1), ((1,), (1,)))[:1])
    half = rows // 2
    message = jnp.concatenate([x[:, at : at + half] for x in lines for at in (0, half)], axis=0)
    for d in range(stat_ref.shape[0]):
        stat_ref[d] = message


def middle_kernel(
    v_ref,
    prior_value_ref,
    scaled_ref,
    prob_ref,
    att_ref,
    stat_ref,
    grad_ref,
    low_ref,
    table_ref,
    *,
    full_width,
):
    rows, width = v_ref.shape
    heads, pairs = width // HEAD_DIM, rows // PAIR
    summed = stat_ref[0]
    for d in range(1, stat_ref.shape[0]):
        summed = summed + stat_ref[d]
    pick = lax.broadcasted_iota(jnp.int32, (4, 4 * HEAD_DIM), 1) // HEAD_DIM
    pick = (pick == lax.broadcasted_iota(jnp.int32, (4, 4 * HEAD_DIM), 0)).astype(f32)
    spread = dot(summed, pick, ((0,), (0,)), exact)
    squares = jnp.concatenate([spread[:, :128], spread[:, 128:256]], axis=0)
    products = jnp.concatenate([spread[:, 256:384], spread[:, 384:]], axis=0)
    inv_rms = lax.rsqrt(squares * (1.0 / full_width) + epsilon)
    pull = inv_rms**3 * (products * (1.0 / full_width))
    lines = []
    for h in range(heads):
        ch = head_of(h)
        grad = (inv_rms * scaled_ref[:, ch] - att_ref[:, ch] * pull).astype(bf16)
        grad_ref[:, ch] = grad
        summed_scores = None
        for g in range(pairs):
            here = rows_of(g)
            prob = prob_ref[h, g]
            values = jnp.concatenate(
                [prior_value_ref[g * PAIR :, ch], v_ref[: (g + 1) * PAIR, ch]], axis=0
            )
            grad_probs = dot(grad[here], values, ((1,), (1,)))
            row_dot = jnp.sum(prob * grad_probs, axis=-1, keepdims=True)
            grad_scores = prob * (grad_probs - row_dot)
            grad_low = grad_scores.astype(bf16)
            low_ref[h, g] = grad_low
            summed_scores = grad_scores if summed_scores is None else summed_scores + grad_scores
        lower = pltpu.roll(summed_scores[SEG:], WINDOW - SEG, 1)
        lines.append(diagonal_sums(summed_scores[:SEG] + lower))
    line = jnp.concatenate(lines, axis=0)
    col = lax.broadcasted_iota(jnp.int32, line.shape, 1)
    wrapped = jnp.sum(jnp.where(col > REL, line, 0.0), axis=1, keepdims=True)
    line = jnp.where(col == 0, line + wrapped, line)
    table_ref[...] = jnp.broadcast_to(line[:, :REL].astype(bf16)[None], table_ref.shape)


def back_kernel(q_ref, prob_ref, grad_ref, low_ref, back_ref):
    rows, width = q_ref.shape
    heads, pairs = width // HEAD_DIM, rows // PAIR
    scale = 1.0 / math.sqrt(HEAD_DIM)
    for h in range(heads):
        ch = head_of(h)
        key_back = []
        value_back = []
        for g in range(pairs):
            here = rows_of(g)
            split = PRIOR - g * PAIR
            key_back.append(dot(low_ref[h, g, :, :split], q_ref[here, ch], ((0,), (0,))))
            prob = prob_ref[h, g, :, :split].astype(bf16)
            value_back.append(dot(prob, grad_ref[here, ch], ((0,), (0,))))
        for parts, back_at, factor in ((key_back, 0, scale), (value_back, PRIOR, 1.0)):
            for g in range(pairs):
                total = sum(
                    (parts[a][(g - a) * PAIR : (g - a + 1) * PAIR] for a in range(1, g + 1)),
                    parts[0][rows_of(g)],
                )
                at = back_at + g * PAIR
                back_ref[at : at + PAIR, ch] = (total * factor).astype(bf16)


def late_kernel(q_ref, k_ref, prior_key_ref, prob_ref, grad_ref, low_ref, dq_ref, dk_ref, dv_ref):
    rows, width = q_ref.shape
    heads, pairs = width // HEAD_DIM, rows // PAIR
    scale = 1.0 / math.sqrt(HEAD_DIM)
    for h in range(heads):
        ch = head_of(h)
        key_own = []
        value_own = []
        for g in range(pairs):
            here = rows_of(g)
            split = PRIOR - g * PAIR
            low = low_ref[h, g]
            keys = jnp.concatenate(
                [prior_key_ref[g * PAIR : PRIOR, ch], k_ref[: (g + 1) * PAIR, ch]], axis=0
            )
            dq_ref[here, ch] = (dot(low, keys, ((1,), (0,))) * scale).astype(bf16)
            key_own.append(dot(low[:, split:], q_ref[here, ch], ((0,), (0,))))
            prob = prob_ref[h, g, :, split:].astype(bf16)
            value_own.append(dot(prob, grad_ref[here, ch], ((0,), (0,))))
        for parts, own_ref, factor in ((key_own, dk_ref, scale), (value_own, dv_ref, 1.0)):
            for g in range(pairs):
                total = sum(
                    (parts[a][rows_of(g)] for a in range(g + 1, pairs)), parts[g][rows_of(g)]
                )
                own_ref[rows_of(g), ch] = total * factor


def final_kernel(dk_ref, dv_ref, back_ref, key_ref, value_ref):
    rows = dk_ref.shape[0]
    key_ref[...] = (dk_ref[...] + back_ref[:rows].astype(f32)).astype(bf16)
    value_ref[...] = (dv_ref[...] + back_ref[rows:].astype(f32)).astype(bf16)


def table_kernel(all_ref, table_ref):
    lines = jnp.sum(all_ref[...].astype(f32), axis=0)
    turn = mirror(REL, REL).astype(bf16)
    table_ref[...] = sum(dot(part, turn, ((1,), (0,))) for part in parts_of(lines, 3)[::-1])


def near(array):
    return pltpu.with_memory_space_constraint(array, pltpu.VMEM)


def far(array):
    return pltpu.with_memory_space_constraint(array, pltpu.HBM)


def call(kernel, outs, *arrays, scalars=0):
    many = isinstance(outs, tuple)
    return pl.pallas_call(
        kernel,
        out_shape=outs,
        in_specs=[SMEM] * scalars + [VMEM] * (len(arrays) - scalars),
        out_specs=(VMEM,) * len(outs) if many else VMEM,
        compiler_params=pltpu.CompilerParams(vmem_limit_bytes=ROOM),
    )(*arrays[:scalars], *(near(a) for a in arrays[scalars:]))


def on_device(queries, key_vectors, value_vectors, cotangent, out_gain, rel_table):
    shape = queries.shape
    rows, width = shape[1], shape[2]
    heads, pairs = width // HEAD_DIM, rows // PAIR
    q, k, v, cot = (a.reshape(rows, width) for a in (queries, key_vectors, value_vectors, cotangent))
    gain = out_gain.reshape(1, width)
    members = lax.axis_size("tp")
    tiles = (heads, pairs, PAIR, WINDOW)
    prior_keys = passed_along(k, SP, 1)
    prior_values = passed_along(v, SP, 1)
    first = (lax.axis_index(SP) == 0).astype(jnp.int32).reshape(1)
    own_block = kept((rows, width), bf16)
    q, k, v, own, bias, scaled = pl.pallas_call(
        early_kernel,
        out_shape=(own_block,) * 3 + (kept(tiles, f32), kept(tiles, f32), kept((rows, width), f32)),
        in_specs=[SMEM, VMEM, VMEM] + [HBM] * 4,
        out_specs=(VMEM,) * 6,
        scratch_shapes=[pltpu.VMEM((rows, width), bf16), pltpu.SemaphoreType.DMA((4,))],
        compiler_params=pltpu.CompilerParams(vmem_limit_bytes=ROOM),
    )(first, near(rel_table), near(gain), *(far(a) for a in (q, k, cot, v)))
    prob, att, stat = call(
        forward_kernel,
        (kept(tiles, f32), kept((rows, width), f32), kept((members, 4, rows // 2), f32)),
        *(q, v, prior_keys, prior_values, own, bias, scaled),
    )
    stat = sent_to_all(stat, "tp")
    grad, low, table = call(
        functools.partial(middle_kernel, full_width=width * members),
        (
            kept((rows, width), bf16),
            kept(tiles, bf16),
            kept((lax.axis_size(SP), heads, REL), bf16),
        ),
        *(v, prior_values, scaled, prob, att, stat),
    )
    table = sent_to_all(table, SP)
    back = call(back_kernel, kept((2 * rows, width), bf16), q, prob, grad, low)
    back = passed_along(back, SP, -1)
    dq, dk, dv = call(
        late_kernel,
        (out((rows, width), bf16), kept((rows, width), f32), kept((rows, width), f32)),
        *(q, k, prior_keys, prob, grad, low),
    )
    grad_keys, grad_values = call(
        final_kernel, (out((rows, width), bf16), out((rows, width), bf16)), dk, dv, back
    )
    grad_table = call(table_kernel, out((heads, REL), f32), table)
    return (dq.reshape(shape), grad_keys.reshape(shape), grad_values.reshape(shape), grad_table)


def solution(mesh):
    finer = Mesh(mesh.devices.reshape(12, 8, mesh.shape["tp"]), ("sp_0", "sp_1", "tp"))
    placed = (
        P(None, SP, "tp"),
        P(None, SP, "tp"),
        P(None, SP, "tp"),
        P(None, SP, "tp"),
        P("tp"),
        P("tp", None),
    )
    return jax.shard_map(
        on_device,
        mesh=finer,
        in_specs=placed,
        out_specs=(P(None, SP, "tp"), P(None, SP, "tp"), P(None, SP, "tp"), P("tp", None)),
        check_vma=False,
    )
```

time: 75.6 us -> 63.4 us (0.84)
  the two profiles are of different devices: /device:TPU:2 before, /device:TPU:8 now
where the time goes in v2:
time: 63.4 us; the launch traced here: 63.1 us
  starting transfers between devices  29.2 us (46%)
  waiting for transfers between devices  16.6 us (26%)
  blocking collectives  7.72 us (12%)
  Pallas kernels  7.58 us (12%)
  local copies, waits for them, and re-layouts  1.33 us (2%)
  between operations  0.71 us (1%)
    all_to_all x1, starting transfers between devices, sent_to_all(): return lax.all_to_all(copies, axis, split_axis=0, concat_axis=0, tiled=True)  19.6 us
    ppermute x3, waiting for transfers between devices, passed_along(): return lax.ppermute(block, axis, route)  13.7 us
    ppermute x3, starting transfers between devices, passed_along(): return lax.ppermute(block, axis, route)  9.56 us
    all_to_all x1, blocking collectives, sent_to_all(): return lax.all_to_all(copies, axis, split_axis=0, concat_axis=0, tiled=True)  7.72 us
    pallas_call x6, Pallas kernels, call(): pl.pallas_call(kernel, out_shape=outs, in_specs=[SMEM] * scalars + [VMEM]...  6.09 us
    all_to_all x1, waiting for transfers between devices, sent_to_all(): return lax.all_to_all(copies, axis, split_axis=0, concat_axis=0, tiled=True)  2.92 us
    pallas_call x1, Pallas kernels, on_device(): pl.pallas_call(early_kernel, out_shape=(own_block,) * 3 + (kept(tiles, f3...  1.49 us
    unnamed x4, local copies, waits for them, and re-layouts  1.33 us
  transfers between devices with their start and end apart: 4, of which 4 were waited for; matrix products, arithmetic and copies ran while one was open for 0% of the time, Pallas kernels for 6%

profile of v2, /device:TPU:8, one launch (start us, length us, event | category | flops | bytes accessed | tf_op | source)
XLA Modules:
  0.0 63.1 jit_solution(6173999335560914367)
XLA Ops:
  0.6 3.5 %collective-permute-start = (bf16[256,256]{1,0:T(8,128)(2,1)}, bf16[256,256]{1,0:T(8,128)(2,1)S(1)}, u32[]{:S(2)}, u32[]{:S(2)}) collective-permute-start(bf16[256,256]{1,0:T(8,128)(2,1)} %bitcast.10), channel_id=1, source_target_pairs={{0,8},{8,16},{16,24},{24,32},{32,40},{40,48},{48,56},{56,64},{64,7... | collective-permute-start | bytes 393224 | tf_op jit(solution)/shard_map/ppermute | solution.py:52
  4.1 3.5 %collective-permute-start.1 = (bf16[256,256]{1,0:T(8,128)(2,1)}, bf16[256,256]{1,0:T(8,128)(2,1)S(1)}, u32[]{:S(2)}, u32[]{:S(2)}) collective-permute-start(bf16[256,256]{1,0:T(8,128)(2,1)} %bitcast.12), channel_id=1, source_target_pairs={{0,8},{8,16},{16,24},{24,32},{32,40},{40,48},{48,56},{56,64},{64,7... | collective-permute-start | bytes 393224 | tf_op jit(solution)/shard_map/ppermute | solution.py:52
  7.6 0.0 copy-start.1
  7.6 0.6 %copy-done.1 = bf16[256]{0:T(256)(128)(2,1)S(1)} copy-done((bf16[256]{0:T(256)(128)(2,1)S(1)}, bf16[256]{0:T(256)(128)(2,1)}, u32[]{:S(2)}) %copy-start.1) | copy-done | bytes 536
  8.3 0.0 copy-start
  8.3 0.7 %copy-done = bf16[2,320]{1,0:T(2,128)(2,1)S(1)} copy-done((bf16[2,320]{1,0:T(2,128)(2,1)S(1)}, bf16[2,320]{1,0:T(2,128)(2,1)}, u32[]{:S(2)}) %copy-start) | copy-done | bytes 1304
  9.0 1.5 %shard_map.93 = (bf16[256,256]{1,0:T(8,128)(2,1)S(1)}, bf16[256,256]{1,0:T(8,128)(2,1)S(1)}, bf16[256,256]{1,0:T(8,128)(2,1)S(1)}, f32[2,2,128,384]{3,2,1,0:T(8,...) custom-call(s32[1]{0:T(128)} %bitcast.first_ref, bf16[2,320]{1,0:T(2,128)(2,1)S(1)} %copy-done, ...), custom_call_target="tpu_custom_call" | custom-call | tf_op jit(solution)/shard_map/pallas_call | solution.py:324
  10.5 4.0 %collective-permute-done.prior_key_ref = bf16[256,256]{1,0:T(8,128)(2,1)S(1)} collective-permute-done((bf16[256,256]{1,0:T(8,128)(2,1)}, bf16[256,256]{1,0:T(8,128)(2,1)S(1)}, u32[]{:S(2)}, u32[]{:S(2)}) %collective-permute-start) | collective-permute-done | bytes 131104 | tf_op jit(solution)/shard_map/ppermute | solution.py:52
  14.5 1.4 %collective-permute-done.1.prior_value_ref = bf16[256,256]{1,0:T(8,128)(2,1)S(1)} collective-permute-done((bf16[256,256]{1,0:T(8,128)(2,1)}, bf16[256,256]{1,0:T(8,128)(2,1)S(1)}, u32[]{:S(2)}, u32[]{:S(2)}) %collective-permute-start.1) | collective-permute-done | bytes 131104 | tf_op jit(solution)/shard_map/ppermute | solution.py:52
  15.9 1.1 %shard_map.94 = (f32[2,2,128,384]{3,2,1,0:T(8,128)S(1)}, f32[256,256]{1,0:T(8,128)S(1)}, f32[8,4,128]{2,1,0:T(4,128)S(1)}) custom-call(bf16[256,256]{1,0:T(8,128)(2,1)S(1)} %get-tuple-element.21.q_ref, bf16[256,256]{1,0:T(8,128)(2,1)S(1)} %get-tuple-element.23.v_ref, bf16[256,256]{1,0:T(8,128)(2,1)S(1)} %collective-permute-done.prior_key_ref, ...), custom_call_target="tpu_custom_call" | custom-call | tf_op jit(solution)/shard_map/pallas_call | solution.py:303
  17.0 7.7 %all_to_all.10.stat_ref = f32[8,4,128]{2,1,0:T(4,128)S(1)} all-to-all(f32[8,4,128]{2,1,0:T(4,128)S(1)} %get-tuple-element.29), channel_id=1, replica_groups=mesh['sp_0'=12,'sp_1'=8,'tp'=8] {'tp'}, dimensions={0} | all-to-all | bytes 32768 | tf_op jit(solution)/shard_map/all_to_all | solution.py:56
  24.8 1.9 %shard_map.95 = (bf16[256,256]{1,0:T(8,128)(2,1)S(1)}, bf16[2,2,128,384]{3,2,1,0:T(8,128)(2,1)S(1)}, bf16[96,2,320]{2,1,0:T(2,128)(2,1)}) custom-call(bf16[256,256]{1,0:T(8,128)(2,1)S(1)} %get-tuple-element.23.v_ref, bf16[256,256]{1,0:T(8,128)(2,1)S(1)} %collective-permute-done.1.prior_value_ref, f32[256,256]{1,0:T(8,128)S(1)} %get-tuple-element.26.scaled_ref, ...), custom_call_target="tpu_custom_call" | custom-call | tf_op jit(solution)/shard_map/pallas_call | solution.py:303
  26.7 19.6 %all-to-all-start.1 = ((bf16[96,2,320]{2,1,0:T(2,128)(2,1)}), bf16[96,2,320]{2,1,0:T(2,128)(2,1)S(1)}, u32[]{:S(2)}, u32[]{:S(2)}) async-start(bf16[96,2,320]{2,1,0:T(2,128)(2,1)} %get-tuple-element.37), calls=%async_computation.1 | async-start | bytes 294912 | tf_op jit(solution)/shard_map/all_to_all | solution.py:56
  46.3 0.3 shard_map.97
  46.6 2.6 %collective-permute-start.2 = (bf16[512,256]{1,0:T(8,128)(2,1)S(1)}, bf16[512,256]{1,0:T(8,128)(2,1)S(1)}, u32[]{:S(2)}, u32[]{:S(2)}) collective-permute-start(bf16[512,256]{1,0:T(8,128)(2,1)S(1)} %shard_map.97), channel_id=1, source_target_pairs={{8,0},{16,8},{24,16},{32,24},{40,32},{48,40},{56,48},{64,56},{72,6... | collective-permute-start | bytes 786440 | tf_op jit(solution)/shard_map/ppermute | solution.py:52
  49.2 1.0 %shard_map.96 = (bf16[256,256]{1,0:T(8,128)(2,1)}, f32[256,256]{1,0:T(8,128)S(1)}, f32[256,256]{1,0:T(8,128)S(1)}) custom-call(bf16[256,256]{1,0:T(8,128)(2,1)S(1)} %get-tuple-element.21.q_ref, bf16[256,256]{1,0:T(8,128)(2,1)S(1)} %get-tuple-element.22.k_ref, bf16[256,256]{1,0:T(8,128)(2,1)S(1)} %collective-permute-done.prior_key_ref, ...), custom_call_target="tpu_custom_call" | custom-call | tf_op jit(solution)/shard_map/pallas_call | solution.py:303
  50.2 8.3 %collective-permute-done.2.back_ref = bf16[512,256]{1,0:T(8,128)(2,1)S(1)} collective-permute-done((bf16[512,256]{1,0:T(8,128)(2,1)S(1)}, bf16[512,256]{1,0:T(8,128)(2,1)S(1)}, u32[]{:S(2)}, u32[]{:S(2)}) %collective-permute-start.2) | collective-permute-done | bytes 262176 | tf_op jit(solution)/shard_map/ppermute | solution.py:52
  58.5 0.7 %shard_map.98 = (bf16[256,256]{1,0:T(8,128)(2,1)}, bf16[256,256]{1,0:T(8,128)(2,1)}) custom-call(f32[256,256]{1,0:T(8,128)S(1)} %get-tuple-element.33.dk_ref, f32[256,256]{1,0:T(8,128)S(1)} %get-tuple-element.34.dv_ref, bf16[512,256]{1,0:T(8,128)(2,1)S(1)} %collective-permute-done.2.back_ref), custom_call_target="tpu_custom_call" | custom-call | tf_op jit(solution)/shard_map/pallas_call | solution.py:303
  59.2 2.9 %all-to-all-done.1.all_ref = bf16[96,2,320]{2,1,0:T(2,128)(2,1)S(1)} async-done(((bf16[96,2,320]{2,1,0:T(2,128)(2,1)}), bf16[96,2,320]{2,1,0:T(2,128)(2,1)S(1)}, u32[]{:S(2)}, u32[]{:S(2)}) %all-to-all-start.1) | async-done | bytes 122912 | tf_op jit(solution)/shard_map/all_to_all | solution.py:56
  62.1 1.0 %shard_map.99 = f32[2,320]{1,0:T(2,128)} custom-call(bf16[96,2,320]{2,1,0:T(2,128)(2,1)S(1)} %all-to-all-done.1.all_ref), custom_call_target="tpu_custom_call" | custom-call | tf_op jit(solution)/shard_map/pallas_call | solution.py:303
  (1 shorter events, 0.0 us)
Async XLA Ops:
  0.6 13.9 %collective-permute-start = (bf16[256,256]{1,0:T(8,128)(2,1)}, bf16[256,256]{1,0:T(8,128)(2,1)S(1)}, u32[]{:S(2)}, u32[]{:S(2)}) collective-permute-start(bf16[256,256]{1,0:T(8,128)(2,1)} %bitcast.10), channel_id=1, source_target_pairs={{0,8},{8,16},{16,24},{24,32},{32,40},{40,48},{48,56},{56,64},{64,7... | collective-permute-start | bytes 393224 | tf_op jit(solution)/shard_map/ppermute | solution.py:52
  4.1 11.8 %collective-permute-start.1 = (bf16[256,256]{1,0:T(8,128)(2,1)}, bf16[256,256]{1,0:T(8,128)(2,1)S(1)}, u32[]{:S(2)}, u32[]{:S(2)}) collective-permute-start(bf16[256,256]{1,0:T(8,128)(2,1)} %bitcast.12), channel_id=1, source_target_pairs={{0,8},{8,16},{16,24},{24,32},{32,40},{40,48},{48,56},{56,64},{64,7... | collective-permute-start | bytes 393224 | tf_op jit(solution)/shard_map/ppermute | solution.py:52
  7.6 0.7 %copy-start.1 = (bf16[256]{0:T(256)(128)(2,1)S(1)}, bf16[256]{0:T(256)(128)(2,1)}, u32[]{:S(2)}) copy-start(bf16[256]{0:T(256)(128)(2,1)} %param.10) | copy-start | bytes 1540
  8.3 0.7 %copy-start = (bf16[2,320]{1,0:T(2,128)(2,1)S(1)}, bf16[2,320]{1,0:T(2,128)(2,1)}, u32[]{:S(2)}) copy-start(bf16[2,320]{1,0:T(2,128)(2,1)} %rel_ref.1) | copy-start | bytes 3844
  26.7 35.4 %all-to-all-start.1 = ((bf16[96,2,320]{2,1,0:T(2,128)(2,1)}), bf16[96,2,320]{2,1,0:T(2,128)(2,1)S(1)}, u32[]{:S(2)}, u32[]{:S(2)}) async-start(bf16[96,2,320]{2,1,0:T(2,128)(2,1)} %get-tuple-element.37), calls=%async_computation.1 | async-start | bytes 294912 | tf_op jit(solution)/shard_map/all_to_all | solution.py:56
  46.6 11.8 %collective-permute-start.2 = (bf16[512,256]{1,0:T(8,128)(2,1)S(1)}, bf16[512,256]{1,0:T(8,128)(2,1)S(1)}, u32[]{:S(2)}, u32[]{:S(2)}) collective-permute-start(bf16[512,256]{1,0:T(8,128)(2,1)S(1)} %shard_map.97), channel_id=1, source_target_pairs={{8,0},{16,8},{24,16},{32,24},{40,32},{48,40},{56,48},{64,56},{72,6... | collective-permute-start | bytes 786440 | tf_op jit(solution)/shard_map/ppermute | solution.py:52

commit v3 on v2

--- a/solution.py
+++ b/solution.py
@@ -6,7 +6,6 @@
 from jax import lax
 from jax.experimental import pallas as pl
 from jax.experimental.pallas import tpu as pltpu
-from jax.sharding import Mesh
 from jax.sharding import PartitionSpec as P
 
 
@@ -14,7 +13,8 @@
 SEG = 64
 LEFT = 4
 REL = 320
-SP = ("sp_0", "sp_1")
+SP = "sp"
+LEADER = (9, 4, 7)
 
 PAIR = 2 * SEG
 PRIOR = LEFT * SEG
@@ -24,7 +24,6 @@
 masked_value = -1e30
 f32 = jnp.float32
 bf16 = jnp.bfloat16
-exact = lax.Precision.HIGHEST
 kept = pltpu.VMEM
 out = jax.ShapeDtypeStruct
 VMEM = pl.BlockSpec(memory_space=pltpu.VMEM)
@@ -32,10 +31,8 @@
 SMEM = pl.BlockSpec(memory_space=pltpu.SMEM)
 
 
-def dot(left, right, dims, precision=None):
-    return lax.dot_general(
-        left, right, (dims, ((), ())), preferred_element_type=f32, precision=precision
-    )
+def dot(left, right, dims):
+    return lax.dot_general(left, right, (dims, ((), ())), preferred_element_type=f32)
 
 
 def parts_of(array, count):
@@ -52,8 +49,14 @@
     return lax.ppermute(block, axis, route)
 
 
-def sent_to_all(copies, axis):
-    return lax.all_to_all(copies, axis, split_axis=0, concat_axis=0, tiled=True)
+def ahead(group, leader):
+    return [group[leader]] + group[:leader] + group[leader + 1 :]
+
+
+def sent_to_all(copies, axis, order):
+    return lax.all_to_all(
+        copies, axis, split_axis=0, concat_axis=0, tiled=True, axis_index_groups=order
+    )
 
 
 def mirror(rows, cols):
@@ -95,6 +98,7 @@
     own_ref,
     bias_ref,
     scaled_ref,
+    turn_ref,
     cot_ref,
     sems,
 ):
@@ -105,6 +109,7 @@
     copies = [pltpu.make_async_copy(a, b, sems.at[i]) for i, (a, b) in enumerate(moves)]
     for copy in copies:
         copy.start()
+    turn_ref[...] = mirror(REL, REL).astype(bf16)
     turned = dot(rel_ref[...], mirror(REL, WINDOW).astype(bf16), ((1,), (0,)))
     row = lax.broadcasted_iota(jnp.int32, (PAIR, WINDOW), 0)
     col = lax.broadcasted_iota(jnp.int32, (PAIR, WINDOW), 1)
@@ -193,9 +198,10 @@
     summed = stat_ref[0]
     for d in range(1, stat_ref.shape[0]):
         summed = summed + stat_ref[d]
-    pick = lax.broadcasted_iota(jnp.int32, (4, 4 * HEAD_DIM), 1) // HEAD_DIM
-    pick = (pick == lax.broadcasted_iota(jnp.int32, (4, 4 * HEAD_DIM), 0)).astype(f32)
-    spread = dot(summed, pick, ((0,), (0,)), exact)
+    pieces = jnp.concatenate(parts_of(summed, 3), axis=0)
+    pick = lax.broadcasted_iota(jnp.int32, (12, 4 * HEAD_DIM), 1) // HEAD_DIM
+    pick = (pick == lax.broadcasted_iota(jnp.int32, (12, 4 * HEAD_DIM), 0) % 4).astype(bf16)
+    spread = dot(pieces, pick, ((0,), (0,)))
     squares = jnp.concatenate([spread[:, :128], spread[:, 128:256]], axis=0)
     products = jnp.concatenate([spread[:, 256:384], spread[:, 384:]], axis=0)
     inv_rms = lax.rsqrt(squares * (1.0 / full_width) + epsilon)
@@ -224,7 +230,7 @@
     col = lax.broadcasted_iota(jnp.int32, line.shape, 1)
     wrapped = jnp.sum(jnp.where(col > REL, line, 0.0), axis=1, keepdims=True)
     line = jnp.where(col == 0, line + wrapped, line)
-    table_ref[...] = jnp.broadcast_to(line[:, :REL].astype(bf16)[None], table_ref.shape)
+    table_ref[...] = jnp.broadcast_to(line[:, :REL][None], table_ref.shape)
 
 
 def back_kernel(q_ref, prob_ref, grad_ref, low_ref, back_ref):
@@ -284,10 +290,15 @@
     value_ref[...] = (dv_ref[...] + back_ref[rows:].astype(f32)).astype(bf16)
 
 
-def table_kernel(all_ref, table_ref):
-    lines = jnp.sum(all_ref[...].astype(f32), axis=0)
-    turn = mirror(REL, REL).astype(bf16)
-    table_ref[...] = sum(dot(part, turn, ((1,), (0,))) for part in parts_of(lines, 3)[::-1])
+def relay_kernel(all_ref, out_ref):
+    out_ref[...] = jnp.broadcast_to(jnp.sum(all_ref[...], axis=0)[None], out_ref.shape)
+
+
+def table_kernel(all_ref, turn_ref, table_ref):
+    heads = table_ref.shape[0]
+    pieces = jnp.concatenate(parts_of(jnp.sum(all_ref[...], axis=0), 3), axis=0)
+    lines = dot(pieces, turn_ref[...], ((1,), (0,)))
+    table_ref[...] = lines[2 * heads :] + lines[heads : 2 * heads] + lines[:heads]
 
 
 def near(array):
@@ -321,11 +332,12 @@
     prior_values = passed_along(v, SP, 1)
     first = (lax.axis_index(SP) == 0).astype(jnp.int32).reshape(1)
     own_block = kept((rows, width), bf16)
-    q, k, v, own, bias, scaled = pl.pallas_call(
+    q, k, v, own, bias, scaled, turn = pl.pallas_call(
         early_kernel,
-        out_shape=(own_block,) * 3 + (kept(tiles, f32), kept(tiles, f32), kept((rows, width), f32)),
+        out_shape=(own_block,) * 3
+        + (kept(tiles, f32), kept(tiles, f32), kept((rows, width), f32), kept((REL, REL), bf16)),
         in_specs=[SMEM, VMEM, VMEM] + [HBM] * 4,
-        out_specs=(VMEM,) * 6,
+        out_specs=(VMEM,) * 7,
         scratch_shapes=[pltpu.VMEM((rows, width), bf16), pltpu.SemaphoreType.DMA((4,))],
         compiler_params=pltpu.CompilerParams(vmem_limit_bytes=ROOM),
     )(first, near(rel_table), near(gain), *(far(a) for a in (q, k, cot, v)))
@@ -334,17 +346,21 @@
         (kept(tiles, f32), kept((rows, width), f32), kept((members, 4, rows // 2), f32)),
         *(q, v, prior_keys, prior_values, own, bias, scaled),
     )
-    stat = sent_to_all(stat, "tp")
+    stat = sent_to_all(stat, "tp", [ahead(list(range(members)), LEADER[2])])
     grad, low, table = call(
         functools.partial(middle_kernel, full_width=width * members),
         (
             kept((rows, width), bf16),
             kept(tiles, bf16),
-            kept((lax.axis_size(SP), heads, REL), bf16),
+            kept((8, heads, REL), f32),
         ),
         *(v, prior_values, scaled, prob, att, stat),
     )
-    table = sent_to_all(table, SP)
+    order = [ahead([z * 8 + y for y in range(8)], LEADER[1]) for z in range(12)]
+    table = sent_to_all(table, SP, order)
+    table = call(relay_kernel, kept((12, heads, REL), f32), table)
+    order = [ahead([z * 8 + y for z in range(12)], LEADER[0]) for y in range(8)]
+    table = sent_to_all(table, SP, order)
     back = call(back_kernel, kept((2 * rows, width), bf16), q, prob, grad, low)
     back = passed_along(back, SP, -1)
     dq, dk, dv = call(
@@ -355,12 +371,11 @@
     grad_keys, grad_values = call(
         final_kernel, (out((rows, width), bf16), out((rows, width), bf16)), dk, dv, back
     )
-    grad_table = call(table_kernel, out((heads, REL), f32), table)
+    grad_table = call(table_kernel, out((heads, REL), f32), table, turn)
     return (dq.reshape(shape), grad_keys.reshape(shape), grad_values.reshape(shape), grad_table)
 
 
 def solution(mesh):
-    finer = Mesh(mesh.devices.reshape(12, 8, mesh.shape["tp"]), ("sp_0", "sp_1", "tp"))
     placed = (
         P(None, SP, "tp"),
         P(None, SP, "tp"),
@@ -371,7 +386,7 @@
     )
     return jax.shard_map(
         on_device,
-        mesh=finer,
+        mesh=mesh,
         in_specs=placed,
         out_specs=(P(None, SP, "tp"), P(None, SP, "tp"), P(None, SP, "tp"), P("tp", None)),
         check_vma=False,

time: 63.4 us -> 62.6 us (0.987)
  blocking collectives: 7.72 us -> 17.4 us
  waiting for transfers between devices: 16.6 us -> 10.9 us
  starting transfers between devices: 29.2 us -> 24.8 us
    all_to_all x1 -> x2, blocking collectives: 7.72 us -> 17.4 us  [sent_to_all(): lax.all_to_all(copies, axis, split_axis=0, concat_axis=0, tiled=True, axi...]
    ppermute x3, waiting for transfers between devices: 13.7 us -> 5.43 us  [passed_along(): return lax.ppermute(block, axis, route)]
    all_to_all x1, starting transfers between devices: 19.6 us -> 15.9 us  [sent_to_all(): lax.all_to_all(copies, axis, split_axis=0, concat_axis=0, tiled=True, axi...]
    all_to_all x1, waiting for transfers between devices: 2.92 us -> 5.44 us  [sent_to_all(): lax.all_to_all(copies, axis, split_axis=0, concat_axis=0, tiled=True, axi...]
    ppermute x3, starting transfers between devices: 9.56 us -> 8.89 us  [passed_along(): return lax.ppermute(block, axis, route)]
    pallas_call x6 -> x7, Pallas kernels: 6.09 us -> 5.62 us  [call(): pl.pallas_call(kernel, out_shape=outs, in_specs=[SMEM] * scalars + [VMEM]...]
  transfers between devices with their start and end apart: 4 -> 4, of which waited for: 4 -> 3; matrix products, arithmetic and copies ran while one was open for 0% -> 0% of each run, Pallas kernels for 6% -> 6%
where the time goes in v3:
time: 62.6 us; the launch traced here: 62.2 us
  starting transfers between devices  24.8 us (40%)
  blocking collectives  17.4 us (28%)
  waiting for transfers between devices  10.9 us (17%)
  Pallas kernels  7.11 us (11%)
  local copies, waits for them, and re-layouts  1.33 us (2%)
  between operations  0.7 us (1%)
    all_to_all x2, blocking collectives, sent_to_all(): lax.all_to_all(copies, axis, split_axis=0, concat_axis=0, tiled=True, axi...  17.4 us
    all_to_all x1, starting transfers between devices, sent_to_all(): lax.all_to_all(copies, axis, split_axis=0, concat_axis=0, tiled=True, axi...  15.9 us
    ppermute x3, starting transfers between devices, passed_along(): return lax.ppermute(block, axis, route)  8.89 us
    pallas_call x7, Pallas kernels, call(): pl.pallas_call(kernel, out_shape=outs, in_specs=[SMEM] * scalars + [VMEM]...  5.62 us
    all_to_all x1, waiting for transfers between devices, sent_to_all(): lax.all_to_all(copies, axis, split_axis=0, concat_axis=0, tiled=True, axi...  5.44 us
    ppermute x3, waiting for transfers between devices, passed_along(): return lax.ppermute(block, axis, route)  5.43 us
    pallas_call x1, Pallas kernels, on_device(): pl.pallas_call(early_kernel, out_shape=(own_block,) * 3 + (kept(tiles, f3...  1.5 us
    unnamed x4, local copies, waits for them, and re-layouts  1.33 us
  transfers between devices with their start and end apart: 4, of which 3 were waited for; matrix products, arithmetic and copies ran while one was open for 0% of the time, Pallas kernels for 6%

profile of v3, /device:TPU:8, one launch (start us, length us, event | category | flops | bytes accessed | tf_op | source)
XLA Modules:
  0.0 62.2 jit_solution(13523627925123490763)
XLA Ops:
  0.6 3.5 %collective-permute-start = (bf16[256,256]{1,0:T(8,128)(2,1)}, bf16[256,256]{1,0:T(8,128)(2,1)S(1)}, u32[]{:S(2)}, u32[]{:S(2)}) collective-permute-start(bf16[256,256]{1,0:T(8,128)(2,1)} %bitcast.10), channel_id=1, source_target_pairs={{0,8},{8,16},{16,24},{24,32},{32,40},{40,48},{48,56},{56,64},{64,7... | collective-permute-start | bytes 393224 | tf_op jit(solution)/shard_map/ppermute | solution.py:49
  4.1 3.5 %collective-permute-start.1 = (bf16[256,256]{1,0:T(8,128)(2,1)}, bf16[256,256]{1,0:T(8,128)(2,1)S(1)}, u32[]{:S(2)}, u32[]{:S(2)}) collective-permute-start(bf16[256,256]{1,0:T(8,128)(2,1)} %bitcast.12), channel_id=1, source_target_pairs={{0,8},{8,16},{16,24},{24,32},{32,40},{40,48},{48,56},{56,64},{64,7... | collective-permute-start | bytes 393224 | tf_op jit(solution)/shard_map/ppermute | solution.py:49
  7.6 0.0 copy-start.1
  7.6 0.6 %copy-done.1 = bf16[256]{0:T(256)(128)(2,1)S(1)} copy-done((bf16[256]{0:T(256)(128)(2,1)S(1)}, bf16[256]{0:T(256)(128)(2,1)}, u32[]{:S(2)}) %copy-start.1) | copy-done | bytes 536
  8.3 0.0 copy-start
  8.3 0.7 %copy-done = bf16[2,320]{1,0:T(2,128)(2,1)S(1)} copy-done((bf16[2,320]{1,0:T(2,128)(2,1)S(1)}, bf16[2,320]{1,0:T(2,128)(2,1)}, u32[]{:S(2)}) %copy-start) | copy-done | bytes 1304
  9.0 1.5 %shard_map.93 = (bf16[256,256]{1,0:T(8,128)(2,1)S(1)}, bf16[256,256]{1,0:T(8,128)(2,1)S(1)}, bf16[256,256]{1,0:T(8,128)(2,1)S(1)}, f32[2,2,128,384]{3,2,1,0:T(8,...) custom-call(s32[1]{0:T(128)} %bitcast.first_ref, ...), custom_call_target="tpu_custom_call" | custom-call | tf_op jit(solution)/shard_map/pallas_call | solution.py:335
  10.5 4.0 %collective-permute-done.prior_key_ref = bf16[256,256]{1,0:T(8,128)(2,1)S(1)} collective-permute-done((bf16[256,256]{1,0:T(8,128)(2,1)}, bf16[256,256]{1,0:T(8,128)(2,1)S(1)}, u32[]{:S(2)}, u32[]{:S(2)}) %collective-permute-start) | collective-permute-done | bytes 131104 | tf_op jit(solution)/shard_map/ppermute | solution.py:49
  14.5 1.4 %collective-permute-done.1.prior_value_ref = bf16[256,256]{1,0:T(8,128)(2,1)S(1)} collective-permute-done((bf16[256,256]{1,0:T(8,128)(2,1)}, bf16[256,256]{1,0:T(8,128)(2,1)S(1)}, u32[]{:S(2)}, u32[]{:S(2)}) %collective-permute-start.1) | collective-permute-done | bytes 131104 | tf_op jit(solution)/shard_map/ppermute | solution.py:49
  15.9 1.1 %shard_map.94 = (f32[2,2,128,384]{3,2,1,0:T(8,128)S(1)}, f32[256,256]{1,0:T(8,128)S(1)}, f32[8,4,128]{2,1,0:T(4,128)S(1)}) custom-call(bf16[256,256]{1,0:T(8,128)(2,1)S(1)} %get-tuple-element.22.q_ref, bf16[256,256]{1,0:T(8,128)(2,1)S(1)} %get-tuple-element.24.v_ref, bf16[256,256]{1,0:T(8,128)(2,1)S(1)} %collective-permute-done.prior_key_ref, ...), custom_call_target="tpu_custom_call" | custom-call | tf_op jit(solution)/shard_map/pallas_call | solution.py:314
  17.0 7.3 %all_to_all.15.stat_ref = f32[8,4,128]{2,1,0:T(4,128)S(1)} all-to-all(f32[8,4,128]{2,1,0:T(4,128)S(1)} %get-tuple-element.30), channel_id=1, replica_groups={{7,0,1,2,3,4,5,6},{15,8,9,10,11,12,13,14},{23,16,17,18,19,20,21,22},{31..., dimensions={0} | all-to-all | bytes 32768 | tf_op jit(solution)/shard_map/all_to_all | solution.py:57
  24.4 1.1 %shard_map.95 = (bf16[256,256]{1,0:T(8,128)(2,1)S(1)}, bf16[2,2,128,384]{3,2,1,0:T(8,128)(2,1)S(1)}, f32[8,2,320]{2,1,0:T(2,128)S(1)}) custom-call(bf16[256,256]{1,0:T(8,128)(2,1)S(1)} %get-tuple-element.24.v_ref, bf16[256,256]{1,0:T(8,128)(2,1)S(1)} %collective-permute-done.1.prior_value_ref, f32[256,256]{1,0:T(8,128)S(1)} %get-tuple-element.27.scaled_ref, ...), custom_call_target="tpu_custom_call" | custom-call | tf_op jit(solution)/shard_map/pallas_call | solution.py:314
  25.4 0.3 shard_map.97
  25.7 1.9 %collective-permute-start.2 = (bf16[512,256]{1,0:T(8,128)(2,1)S(1)}, bf16[512,256]{1,0:T(8,128)(2,1)S(1)}, u32[]{:S(2)}, u32[]{:S(2)}) collective-permute-start(bf16[512,256]{1,0:T(8,128)(2,1)S(1)} %shard_map.97), channel_id=1, source_target_pairs={{8,0},{16,8},{24,16},{32,24},{40,32},{48,40},{56,48},{64,56},{72,6... | collective-permute-start | bytes 786440 | tf_op jit(solution)/shard_map/ppermute | solution.py:49
  27.7 10.1 %all_to_all.16.all_ref = f32[8,2,320]{2,1,0:T(2,128)S(1)} all-to-all(f32[8,2,320]{2,1,0:T(2,128)S(1)} %get-tuple-element.38), channel_id=1, replica_groups={{32,0,8,16,24,40,48,56},{96,64,72,80,88,104,112,120},{160,128,136,144,1..., dimensions={0} | all-to-all | bytes 40960 | tf_op jit(solution)/shard_map/all_to_all | solution.py:57
  37.8 0.6 %shard_map.99 = f32[12,2,320]{2,1,0:T(2,128)} custom-call(f32[8,2,320]{2,1,0:T(2,128)S(1)} %all_to_all.16.all_ref), custom_call_target="tpu_custom_call" | custom-call | tf_op jit(solution)/shard_map/pallas_call | solution.py:314
  38.4 15.9 %all-to-all-start.2 = ((f32[12,2,320]{2,1,0:T(2,128)}), f32[12,2,320]{2,1,0:T(2,128)S(1)}, u32[]{:S(2)}, u32[]{:S(2)}) async-start(f32[12,2,320]{2,1,0:T(2,128)} %shard_map.99), calls=%async_computation.2 | async-start | bytes 73728 | tf_op jit(solution)/shard_map/all_to_all | solution.py:57
  54.3 1.0 %shard_map.96 = (bf16[256,256]{1,0:T(8,128)(2,1)}, f32[256,256]{1,0:T(8,128)S(1)}, f32[256,256]{1,0:T(8,128)S(1)}) custom-call(bf16[256,256]{1,0:T(8,128)(2,1)S(1)} %get-tuple-element.22.q_ref, bf16[256,256]{1,0:T(8,128)(2,1)S(1)} %get-tuple-element.23.k_ref, bf16[256,256]{1,0:T(8,128)(2,1)S(1)} %collective-permute-done.prior_key_ref, ...), custom_call_target="tpu_custom_call" | custom-call | tf_op jit(solution)/shard_map/pallas_call | solution.py:314
  55.3 5.4 %all-to-all-done.2.all_ref = f32[12,2,320]{2,1,0:T(2,128)S(1)} async-done(((f32[12,2,320]{2,1,0:T(2,128)}), f32[12,2,320]{2,1,0:T(2,128)S(1)}, u32[]{:S(2)}, u32[]{:S(2)}) %all-to-all-start.2) | async-done | bytes 30752 | tf_op jit(solution)/shard_map/all_to_all | solution.py:57
  60.8 0.8 %shard_map.100 = f32[2,320]{1,0:T(2,128)} custom-call(f32[12,2,320]{2,1,0:T(2,128)S(1)} %all-to-all-done.2.all_ref, bf16[320,320]{1,0:T(8,128)(2,1)S(1)} %get-tuple-element.39.turn_ref), custom_call_target="tpu_custom_call" | custom-call | tf_op jit(solution)/shard_map/pallas_call | solution.py:314
  61.5 0.0 collective-permute-done.2.back_ref
  61.5 0.7 %shard_map.98 = (bf16[256,256]{1,0:T(8,128)(2,1)}, bf16[256,256]{1,0:T(8,128)(2,1)}) custom-call(f32[256,256]{1,0:T(8,128)S(1)} %get-tuple-element.34.dk_ref, f32[256,256]{1,0:T(8,128)S(1)} %get-tuple-element.35.dv_ref, bf16[512,256]{1,0:T(8,128)(2,1)S(1)} %collective-permute-done.2.back_ref), custom_call_target="tpu_custom_call" | custom-call | tf_op jit(solution)/shard_map/pallas_call | solution.py:314
  (1 shorter events, 0.0 us)
Async XLA Ops:
  0.6 13.9 %collective-permute-start = (bf16[256,256]{1,0:T(8,128)(2,1)}, bf16[256,256]{1,0:T(8,128)(2,1)S(1)}, u32[]{:S(2)}, u32[]{:S(2)}) collective-permute-start(bf16[256,256]{1,0:T(8,128)(2,1)} %bitcast.10), channel_id=1, source_target_pairs={{0,8},{8,16},{16,24},{24,32},{32,40},{40,48},{48,56},{56,64},{64,7... | collective-permute-start | bytes 393224 | tf_op jit(solution)/shard_map/ppermute | solution.py:49
  4.1 11.8 %collective-permute-start.1 = (bf16[256,256]{1,0:T(8,128)(2,1)}, bf16[256,256]{1,0:T(8,128)(2,1)S(1)}, u32[]{:S(2)}, u32[]{:S(2)}) collective-permute-start(bf16[256,256]{1,0:T(8,128)(2,1)} %bitcast.12), channel_id=1, source_target_pairs={{0,8},{8,16},{16,24},{24,32},{32,40},{40,48},{48,56},{56,64},{64,7... | collective-permute-start | bytes 393224 | tf_op jit(solution)/shard_map/ppermute | solution.py:49
  7.6 0.7 %copy-start.1 = (bf16[256]{0:T(256)(128)(2,1)S(1)}, bf16[256]{0:T(256)(128)(2,1)}, u32[]{:S(2)}) copy-start(bf16[256]{0:T(256)(128)(2,1)} %param.10) | copy-start | bytes 1540
  8.3 0.7 %copy-start = (bf16[2,320]{1,0:T(2,128)(2,1)S(1)}, bf16[2,320]{1,0:T(2,128)(2,1)}, u32[]{:S(2)}) copy-start(bf16[2,320]{1,0:T(2,128)(2,1)} %rel_ref.1) | copy-start | bytes 3844
  25.7 35.8 %collective-permute-start.2 = (bf16[512,256]{1,0:T(8,128)(2,1)S(1)}, bf16[512,256]{1,0:T(8,128)(2,1)S(1)}, u32[]{:S(2)}, u32[]{:S(2)}) collective-permute-start(bf16[512,256]{1,0:T(8,128)(2,1)S(1)} %shard_map.97), channel_id=1, source_target_pairs={{8,0},{16,8},{24,16},{32,24},{40,32},{48,40},{56,48},{64,56},{72,6... | collective-permute-start | bytes 786440 | tf_op jit(solution)/shard_map/ppermute | solution.py:49
  38.4 22.3 %all-to-all-start.2 = ((f32[12,2,320]{2,1,0:T(2,128)}), f32[12,2,320]{2,1,0:T(2,128)S(1)}, u32[]{:S(2)}, u32[]{:S(2)}) async-start(f32[12,2,320]{2,1,0:T(2,128)} %shard_map.99), calls=%async_computation.2 | async-start | bytes 73728 | tf_op jit(solution)/shard_map/all_to_all | solution.py:57

commit v4 on v3

--- a/solution.py
+++ b/solution.py
@@ -138,34 +138,38 @@
     copies[3].wait()
 
 
-def forward_kernel(
-    q_ref, v_ref, prior_key_ref, prior_value_ref, own_ref, bias_ref, scaled_ref, prob_ref, att_ref, stat_ref
-):
-    rows, width = q_ref.shape
-    heads, pairs = width // HEAD_DIM, rows // PAIR
+def weights_kernel(q_ref, prior_key_ref, own_ref, bias_ref, prob_ref, weight_ref):
+    heads, pairs = prob_ref.shape[:2]
     scale = 1.0 / math.sqrt(HEAD_DIM)
-    squares = None
-    products = None
-    for h in range(heads):
-        ch = head_of(h)
-        outs = []
-        for g in range(pairs):
-            here = rows_of(g)
-            split = PRIOR - g * PAIR
-            scores = dot(q_ref[here, ch], prior_key_ref[g * PAIR : PRIOR, ch], ((1,), (1,)))
+    for h in range(heads):
+        for g in range(pairs):
+            split = PRIOR - g * PAIR
+            keys = prior_key_ref[g * PAIR : PRIOR, head_of(h)]
+            scores = dot(q_ref[rows_of(g), head_of(h)], keys, ((1,), (1,)))
             scores = scores * scale + bias_ref[h, g, :, :split]
             scores = jnp.concatenate([scores, own_ref[h, g, :, split:]], axis=1)
             top = jnp.max(scores, axis=-1, keepdims=True)
             shifted = jnp.exp(scores - top)
             prob = shifted * (1.0 / jnp.sum(shifted, axis=-1, keepdims=True))
             prob_ref[h, g] = prob
+            weight_ref[h, g] = prob.astype(bf16)
+
+
+def forward_kernel(weight_ref, v_ref, prior_value_ref, scaled_ref, att_ref, stat_ref):
+    rows, width = v_ref.shape
+    heads, pairs = width // HEAD_DIM, rows // PAIR
+    squares = None
+    products = None
+    for h in range(heads):
+        ch = head_of(h)
+        outs = []
+        for g in range(pairs):
             values = jnp.concatenate(
                 [prior_value_ref[g * PAIR :, ch], v_ref[: (g + 1) * PAIR, ch]], axis=0
             )
-            attended = dot(prob.astype(bf16), values, ((1,), (0,)))
-            att_ref[here, ch] = attended
-            outs.append(attended)
+            outs.append(dot(weight_ref[h, g], values, ((1,), (0,))))
         attended = jnp.concatenate(outs, axis=0)
+        att_ref[:, ch] = attended
         square = attended * attended
         product = attended * scaled_ref[:, ch]
         squares = square if squares is None else squares + square
@@ -233,7 +237,7 @@
     table_ref[...] = jnp.broadcast_to(line[:, :REL][None], table_ref.shape)
 
 
-def back_kernel(q_ref, prob_ref, grad_ref, low_ref, back_ref):
+def back_kernel(q_ref, weight_ref, grad_ref, low_ref, back_ref):
     rows, width = q_ref.shape
     heads, pairs = width // HEAD_DIM, rows // PAIR
     scale = 1.0 / math.sqrt(HEAD_DIM)
@@ -245,8 +249,7 @@
             here = rows_of(g)
             split = PRIOR - g * PAIR
             key_back.append(dot(low_ref[h, g, :, :split], q_ref[here, ch], ((0,), (0,))))
-            prob = prob_ref[h, g, :, :split].astype(bf16)
-            value_back.append(dot(prob, grad_ref[here, ch], ((0,), (0,))))
+            value_back.append(dot(weight_ref[h, g, :, :split], grad_ref[here, ch], ((0,), (0,))))
         for parts, back_at, factor in ((key_back, 0, scale), (value_back, PRIOR, 1.0)):
             for g in range(pairs):
                 total = sum(
@@ -257,7 +260,7 @@
                 back_ref[at : at + PAIR, ch] = (total * factor).astype(bf16)
 
 
-def late_kernel(q_ref, k_ref, prior_key_ref, prob_ref, grad_ref, low_ref, dq_ref, dk_ref, dv_ref):
+def late_kernel(q_ref, k_ref, prior_key_ref, weight_ref, grad_ref, low_ref, dq_ref, dk_ref, dv_ref):
     rows, width = q_ref.shape
     heads, pairs = width // HEAD_DIM, rows // PAIR
     scale = 1.0 / math.sqrt(HEAD_DIM)
@@ -274,8 +277,7 @@
             )
             dq_ref[here, ch] = (dot(low, keys, ((1,), (0,))) * scale).astype(bf16)
             key_own.append(dot(low[:, split:], q_ref[here, ch], ((0,), (0,))))
-            prob = prob_ref[h, g, :, split:].astype(bf16)
-            value_own.append(dot(prob, grad_ref[here, ch], ((0,), (0,))))
+            value_own.append(dot(weight_ref[h, g, :, split:], grad_ref[here, ch], ((0,), (0,))))
         for parts, own_ref, factor in ((key_own, dk_ref, scale), (value_own, dv_ref, 1.0)):
             for g in range(pairs):
                 total = sum(
@@ -284,21 +286,18 @@
                 own_ref[rows_of(g), ch] = total * factor
 
 
-def final_kernel(dk_ref, dv_ref, back_ref, key_ref, value_ref):
+def final_kernel(dk_ref, dv_ref, back_ref, all_ref, turn_ref, key_ref, value_ref, table_ref):
     rows = dk_ref.shape[0]
+    heads = table_ref.shape[0]
     key_ref[...] = (dk_ref[...] + back_ref[:rows].astype(f32)).astype(bf16)
     value_ref[...] = (dv_ref[...] + back_ref[rows:].astype(f32)).astype(bf16)
-
-
-def relay_kernel(all_ref, out_ref):
-    out_ref[...] = jnp.broadcast_to(jnp.sum(all_ref[...], axis=0)[None], out_ref.shape)
-
-
-def table_kernel(all_ref, turn_ref, table_ref):
-    heads = table_ref.shape[0]
     pieces = jnp.concatenate(parts_of(jnp.sum(all_ref[...], axis=0), 3), axis=0)
     lines = dot(pieces, turn_ref[...], ((1,), (0,)))
     table_ref[...] = lines[2 * heads :] + lines[heads : 2 * heads] + lines[:heads]
+
+
+def relay_kernel(all_ref, out_ref):
+    out_ref[...] = jnp.broadcast_to(jnp.sum(all_ref[...], axis=0)[None], out_ref.shape)
 
 
 def near(array):
@@ -341,10 +340,13 @@
         scratch_shapes=[pltpu.VMEM((rows, width), bf16), pltpu.SemaphoreType.DMA((4,))],
         compiler_params=pltpu.CompilerParams(vmem_limit_bytes=ROOM),
     )(first, near(rel_table), near(gain), *(far(a) for a in (q, k, cot, v)))
-    prob, att, stat = call(
+    prob, weight = call(
+        weights_kernel, (kept(tiles, f32), kept(tiles, bf16)), q, prior_keys, own, bias
+    )
+    att, stat = call(
         forward_kernel,
-        (kept(tiles, f32), kept((rows, width), f32), kept((members, 4, rows // 2), f32)),
-        *(q, v, prior_keys, prior_values, own, bias, scaled),
+        (kept((rows, width), f32), kept((members, 4, rows // 2), f32)),
+        *(weight, v, prior_values, scaled),
     )
     stat = sent_to_all(stat, "tp", [ahead(list(range(members)), LEADER[2])])
     grad, low, table = call(
@@ -352,26 +354,27 @@
         (
             kept((rows, width), bf16),
             kept(tiles, bf16),
-            kept((8, heads, REL), f32),
+            kept((12, heads, REL), f32),
         ),
         *(v, prior_values, scaled, prob, att, stat),
     )
+    order = [ahead([z * 8 + y for z in range(12)], LEADER[0]) for y in range(8)]
+    table = sent_to_all(table, SP, order)
+    table = call(relay_kernel, kept((8, heads, REL), f32), table)
     order = [ahead([z * 8 + y for y in range(8)], LEADER[1]) for z in range(12)]
     table = sent_to_all(table, SP, order)
-    table = call(relay_kernel, kept((12, heads, REL), f32), table)
-    order = [ahead([z * 8 + y for z in range(12)], LEADER[0]) for y in range(8)]
-    table = sent_to_all(table, SP, order)
-    back = call(back_kernel, kept((2 * rows, width), bf16), q, prob, grad, low)
+    back = call(back_kernel, kept((2 * rows, width), bf16), q, weight, grad, low)
     back = passed_along(back, SP, -1)
     dq, dk, dv = call(
         late_kernel,
         (out((rows, width), bf16), kept((rows, width), f32), kept((rows, width), f32)),
-        *(q, k, prior_keys, prob, grad, low),
-    )
-    grad_keys, grad_values = call(
-        final_kernel, (out((rows, width), bf16), out((rows, width), bf16)), dk, dv, back
-    )
-    grad_table = call(table_kernel, out((heads, REL), f32), table, turn)
+        *(q, k, prior_keys, weight, grad, low),
+    )
+    grad_keys, grad_values, grad_table = call(
+        final_kernel,
+        (out((rows, width), bf16), out((rows, width), bf16), out((heads, REL), f32)),
+        *(dk, dv, back, table, turn),
+    )
     return (dq.reshape(shape), grad_keys.reshape(shape), grad_values.reshape(shape), grad_table)
 
 

time: 62.6 us -> 60.8 us (0.971)
  blocking collectives: 17.4 us -> 28.7 us
  starting transfers between devices: 24.8 us -> 16.1 us
  waiting for transfers between devices: 10.9 us -> 7.48 us
  Pallas kernels: 7.11 us -> 6.11 us
    all_to_all x2, blocking collectives: 17.4 us -> 28.7 us  [sent_to_all(): lax.all_to_all(copies, axis, split_axis=0, concat_axis=0, tiled=True, axi...]
    all_to_all x1, starting transfers between devices: 15.9 us -> 7.15 us  [sent_to_all(): lax.all_to_all(copies, axis, split_axis=0, concat_axis=0, tiled=True, axi...]
    all_to_all x1, waiting for transfers between devices: 5.44 us -> 2.49 us  [sent_to_all(): lax.all_to_all(copies, axis, split_axis=0, concat_axis=0, tiled=True, axi...]
    pallas_call x7, Pallas kernels: 5.62 us -> 4.62 us  [call(): pl.pallas_call(kernel, out_shape=outs, in_specs=[SMEM] * scalars + [VMEM]...]
where the time goes in v4:
time: 60.8 us; the launch traced here: 60.4 us
  blocking collectives  28.7 us (47%)
  starting transfers between devices  16.1 us (26%)
  waiting for transfers between devices  7.48 us (12%)
  Pallas kernels  6.11 us (10%)
  local copies, waits for them, and re-layouts  1.33 us (2%)
  between operations  0.7 us (1%)
    all_to_all x2, blocking collectives, sent_to_all(): lax.all_to_all(copies, axis, split_axis=0, concat_axis=0, tiled=True, axi...  28.7 us
    ppermute x3, starting transfers between devices, passed_along(): return lax.ppermute(block, axis, route)  8.99 us
    all_to_all x1, starting transfers between devices, sent_to_all(): lax.all_to_all(copies, axis, split_axis=0, concat_axis=0, tiled=True, axi...  7.15 us
    ppermute x3, waiting for transfers between devices, passed_along(): return lax.ppermute(block, axis, route)  4.99 us
    pallas_call x7, Pallas kernels, call(): pl.pallas_call(kernel, out_shape=outs, in_specs=[SMEM] * scalars + [VMEM]...  4.62 us
    all_to_all x1, waiting for transfers between devices, sent_to_all(): lax.all_to_all(copies, axis, split_axis=0, concat_axis=0, tiled=True, axi...  2.49 us
    pallas_call x1, Pallas kernels, on_device(): pl.pallas_call(early_kernel, out_shape=(own_block,) * 3 + (kept(tiles, f3...  1.5 us
    unnamed x4, local copies, waits for them, and re-layouts  1.33 us
  transfers between devices with their start and end apart: 4, of which 3 were waited for; matrix products, arithmetic and copies ran while one was open for 0% of the time, Pallas kernels for 6%

profile of v4, /device:TPU:8, one launch (start us, length us, event | category | flops | bytes accessed | tf_op | source)
XLA Modules:
  0.0 60.4 jit_solution(13841637172256746605)
XLA Ops:
  0.6 3.5 %collective-permute-start = (bf16[256,256]{1,0:T(8,128)(2,1)}, bf16[256,256]{1,0:T(8,128)(2,1)S(1)}, u32[]{:S(2)}, u32[]{:S(2)}) collective-permute-start(bf16[256,256]{1,0:T(8,128)(2,1)} %bitcast.10), channel_id=1, source_target_pairs={{0,8},{8,16},{16,24},{24,32},{32,40},{40,48},{48,56},{56,64},{64,7... | collective-permute-start | bytes 393224 | tf_op jit(solution)/shard_map/ppermute | solution.py:49
  4.1 3.5 %collective-permute-start.1 = (bf16[256,256]{1,0:T(8,128)(2,1)}, bf16[256,256]{1,0:T(8,128)(2,1)S(1)}, u32[]{:S(2)}, u32[]{:S(2)}) collective-permute-start(bf16[256,256]{1,0:T(8,128)(2,1)} %bitcast.12), channel_id=1, source_target_pairs={{0,8},{8,16},{16,24},{24,32},{32,40},{40,48},{48,56},{56,64},{64,7... | collective-permute-start | bytes 393224 | tf_op jit(solution)/shard_map/ppermute | solution.py:49
  7.6 0.0 copy-start.1
  7.6 0.6 %copy-done.1 = bf16[256]{0:T(256)(128)(2,1)S(1)} copy-done((bf16[256]{0:T(256)(128)(2,1)S(1)}, bf16[256]{0:T(256)(128)(2,1)}, u32[]{:S(2)}) %copy-start.1) | copy-done | bytes 536
  8.3 0.0 copy-start
  8.3 0.7 %copy-done = bf16[2,320]{1,0:T(2,128)(2,1)S(1)} copy-done((bf16[2,320]{1,0:T(2,128)(2,1)S(1)}, bf16[2,320]{1,0:T(2,128)(2,1)}, u32[]{:S(2)}) %copy-start) | copy-done | bytes 1304
  9.0 1.5 %shard_map.93 = (bf16[256,256]{1,0:T(8,128)(2,1)S(1)}, bf16[256,256]{1,0:T(8,128)(2,1)S(1)}, bf16[256,256]{1,0:T(8,128)(2,1)S(1)}, f32[2,2,128,384]{3,2,1,0:T(8,...) custom-call(s32[1]{0:T(128)} %bitcast.first_ref, ...), custom_call_target="tpu_custom_call" | custom-call | tf_op jit(solution)/shard_map/pallas_call | solution.py:334
  10.5 4.0 %collective-permute-done.prior_key_ref = bf16[256,256]{1,0:T(8,128)(2,1)S(1)} collective-permute-done((bf16[256,256]{1,0:T(8,128)(2,1)}, bf16[256,256]{1,0:T(8,128)(2,1)S(1)}, u32[]{:S(2)}, u32[]{:S(2)}) %collective-permute-start) | collective-permute-done | bytes 131104 | tf_op jit(solution)/shard_map/ppermute | solution.py:49
  14.5 0.4 shard_map.94
  14.9 1.0 %collective-permute-done.1.prior_value_ref = bf16[256,256]{1,0:T(8,128)(2,1)S(1)} collective-permute-done((bf16[256,256]{1,0:T(8,128)(2,1)}, bf16[256,256]{1,0:T(8,128)(2,1)S(1)}, u32[]{:S(2)}, u32[]{:S(2)}) %collective-permute-start.1) | collective-permute-done | bytes 131104 | tf_op jit(solution)/shard_map/ppermute | solution.py:49
  15.9 0.4 shard_map.95
  16.3 7.3 %all_to_all.15.stat_ref = f32[8,4,128]{2,1,0:T(4,128)S(1)} all-to-all(f32[8,4,128]{2,1,0:T(4,128)S(1)} %get-tuple-element.33), channel_id=1, replica_groups={{7,0,1,2,3,4,5,6},{15,8,9,10,11,12,13,14},{23,16,17,18,19,20,21,22},{31..., dimensions={0} | all-to-all | bytes 32768 | tf_op jit(solution)/shard_map/all_to_all | solution.py:57
  23.6 1.1 %shard_map.96 = (bf16[256,256]{1,0:T(8,128)(2,1)S(1)}, bf16[2,2,128,384]{3,2,1,0:T(8,128)(2,1)S(1)}, f32[12,2,320]{2,1,0:T(2,128)S(1)}) custom-call(bf16[256,256]{1,0:T(8,128)(2,1)S(1)} %get-tuple-element.29.v_ref, bf16[256,256]{1,0:T(8,128)(2,1)S(1)} %collective-permute-done.1.prior_value_ref, f32[256,256]{1,0:T(8,128)S(1)} %get-tuple-element.30.scaled_ref, ...), custom_call_target="tpu_custom_call" | custom-call | tf_op jit(solution)/shard_map/pallas_call | solution.py:313
  24.7 0.3 shard_map.98
  25.0 2.0 %collective-permute-start.2 = (bf16[512,256]{1,0:T(8,128)(2,1)S(1)}, bf16[512,256]{1,0:T(8,128)(2,1)S(1)}, u32[]{:S(2)}, u32[]{:S(2)}) collective-permute-start(bf16[512,256]{1,0:T(8,128)(2,1)S(1)} %shard_map.98), channel_id=1, source_target_pairs={{8,0},{16,8},{24,16},{32,24},{40,32},{48,40},{56,48},{64,56},{72,6... | collective-permute-start | bytes 786440 | tf_op jit(solution)/shard_map/ppermute | solution.py:49
  27.0 21.3 %all_to_all.16.all_ref = f32[12,2,320]{2,1,0:T(2,128)S(1)} all-to-all(f32[12,2,320]{2,1,0:T(2,128)S(1)} %get-tuple-element.39), channel_id=1, replica_groups={{576,0,64,128,192,256,320,384,448,512,640,704},{584,8,72,136,200,264,32..., dimensions={0} | all-to-all | bytes 61440 | tf_op jit(solution)/shard_map/all_to_all | solution.py:57
  48.4 0.6 %shard_map.99 = f32[8,2,320]{2,1,0:T(2,128)} custom-call(f32[12,2,320]{2,1,0:T(2,128)S(1)} %all_to_all.16.all_ref), custom_call_target="tpu_custom_call" | custom-call | tf_op jit(solution)/shard_map/pallas_call | solution.py:313
  49.0 7.2 %all-to-all-start.2 = ((f32[8,2,320]{2,1,0:T(2,128)}), f32[8,2,320]{2,1,0:T(2,128)S(1)}, u32[]{:S(2)}, u32[]{:S(2)}) async-start(f32[8,2,320]{2,1,0:T(2,128)} %shard_map.99), calls=%async_computation.2 | async-start | bytes 49152 | tf_op jit(solution)/shard_map/all_to_all | solution.py:57
  56.2 1.0 %shard_map.97 = (bf16[256,256]{1,0:T(8,128)(2,1)}, f32[256,256]{1,0:T(8,128)S(1)}, f32[256,256]{1,0:T(8,128)S(1)}) custom-call(bf16[256,256]{1,0:T(8,128)(2,1)S(1)} %get-tuple-element.24.q_ref, bf16[256,256]{1,0:T(8,128)(2,1)S(1)} %get-tuple-element.25.k_ref, bf16[256,256]{1,0:T(8,128)(2,1)S(1)} %collective-permute-done.prior_key_ref, ...), custom_call_target="tpu_custom_call" | custom-call | tf_op jit(solution)/shard_map/pallas_call | solution.py:313
  57.1 2.5 %all-to-all-done.2.all_ref = f32[8,2,320]{2,1,0:T(2,128)S(1)} async-done(((f32[8,2,320]{2,1,0:T(2,128)}), f32[8,2,320]{2,1,0:T(2,128)S(1)}, u32[]{:S(2)}, u32[]{:S(2)}) %all-to-all-start.2) | async-done | bytes 20512 | tf_op jit(solution)/shard_map/all_to_all | solution.py:57
  59.6 0.0 collective-permute-done.2.back_ref
  59.6 0.8 %shard_map.100 = (bf16[256,256]{1,0:T(8,128)(2,1)}, bf16[256,256]{1,0:T(8,128)(2,1)}, f32[2,320]{1,0:T(2,128)}) custom-call(f32[256,256]{1,0:T(8,128)S(1)} %get-tuple-element.37.dk_ref, f32[256,256]{1,0:T(8,128)S(1)} %get-tuple-element.38.dv_ref, bf16[512,256]{1,0:T(8,128)(2,1)S(1)} %collective-permute-done.2.back_ref, ...), custom_call_target="tpu_custom_call" | custom-call | tf_op jit(solution)/shard_map/pallas_call | solution.py:313
  (1 shorter events, 0.0 us)
Async XLA Ops:
  0.6 13.9 %collective-permute-start = (bf16[256,256]{1,0:T(8,128)(2,1)}, bf16[256,256]{1,0:T(8,128)(2,1)S(1)}, u32[]{:S(2)}, u32[]{:S(2)}) collective-permute-start(bf16[256,256]{1,0:T(8,128)(2,1)} %bitcast.10), channel_id=1, source_target_pairs={{0,8},{8,16},{16,24},{24,32},{32,40},{40,48},{48,56},{56,64},{64,7... | collective-permute-start | bytes 393224 | tf_op jit(solution)/shard_map/ppermute | solution.py:49
  4.1 11.8 %collective-permute-start.1 = (bf16[256,256]{1,0:T(8,128)(2,1)}, bf16[256,256]{1,0:T(8,128)(2,1)S(1)}, u32[]{:S(2)}, u32[]{:S(2)}) collective-permute-start(bf16[256,256]{1,0:T(8,128)(2,1)} %bitcast.12), channel_id=1, source_target_pairs={{0,8},{8,16},{16,24},{24,32},{32,40},{40,48},{48,56},{56,64},{64,7... | collective-permute-start | bytes 393224 | tf_op jit(solution)/shard_map/ppermute | solution.py:49
  7.6 0.7 %copy-start.1 = (bf16[256]{0:T(256)(128)(2,1)S(1)}, bf16[256]{0:T(256)(128)(2,1)}, u32[]{:S(2)}) copy-start(bf16[256]{0:T(256)(128)(2,1)} %param.10) | copy-start | bytes 1540
  8.3 0.7 %copy-start = (bf16[2,320]{1,0:T(2,128)(2,1)S(1)}, bf16[2,320]{1,0:T(2,128)(2,1)}, u32[]{:S(2)}) copy-start(bf16[2,320]{1,0:T(2,128)(2,1)} %rel_ref.1) | copy-start | bytes 3844
  25.0 34.6 %collective-permute-start.2 = (bf16[512,256]{1,0:T(8,128)(2,1)S(1)}, bf16[512,256]{1,0:T(8,128)(2,1)S(1)}, u32[]{:S(2)}, u32[]{:S(2)}) collective-permute-start(bf16[512,256]{1,0:T(8,128)(2,1)S(1)} %shard_map.98), channel_id=1, source_target_pairs={{8,0},{16,8},{24,16},{32,24},{40,32},{48,40},{56,48},{64,56},{72,6... | collective-permute-start | bytes 786440 | tf_op jit(solution)/shard_map/ppermute | solution.py:49
  49.0 10.6 %all-to-all-start.2 = ((f32[8,2,320]{2,1,0:T(2,128)}), f32[8,2,320]{2,1,0:T(2,128)S(1)}, u32[]{:S(2)}, u32[]{:S(2)}) async-start(f32[8,2,320]{2,1,0:T(2,128)} %shard_map.99), calls=%async_computation.2 | async-start | bytes 49152 | tf_op jit(solution)/shard_map/all_to_all | solution.py:57

commit v5 on v4

--- a/solution.py
+++ b/solution.py
@@ -14,7 +14,7 @@
 LEFT = 4
 REL = 320
 SP = "sp"
-LEADER = (9, 4, 7)
+LEADER = (8, 4, 5)
 
 PAIR = 2 * SEG
 PRIOR = LEFT * SEG
@@ -202,14 +202,14 @@
     summed = stat_ref[0]
     for d in range(1, stat_ref.shape[0]):
         summed = summed + stat_ref[d]
-    pieces = jnp.concatenate(parts_of(summed, 3), axis=0)
+    inv_line = lax.rsqrt(summed[:2] * (1.0 / full_width) + epsilon)
+    pull_line = inv_line**3 * (summed[2:] * (1.0 / full_width))
+    pieces = jnp.concatenate(parts_of(jnp.concatenate([inv_line, pull_line], axis=0), 3), axis=0)
     pick = lax.broadcasted_iota(jnp.int32, (12, 4 * HEAD_DIM), 1) // HEAD_DIM
     pick = (pick == lax.broadcasted_iota(jnp.int32, (12, 4 * HEAD_DIM), 0) % 4).astype(bf16)
     spread = dot(pieces, pick, ((0,), (0,)))
-    squares = jnp.concatenate([spread[:, :128], spread[:, 128:256]], axis=0)
-    products = jnp.concatenate([spread[:, 256:384], spread[:, 384:]], axis=0)
-    inv_rms = lax.rsqrt(squares * (1.0 / full_width) + epsilon)
-    pull = inv_rms**3 * (products * (1.0 / full_width))
+    inv_rms = jnp.concatenate([spread[:, :128], spread[:, 128:256]], axis=0)
+    pull = jnp.concatenate([spread[:, 256:384], spread[:, 384:]], axis=0)
     lines = []
     for h in range(heads):
         ch = head_of(h)

time: 60.8 us -> 60 us (0.987)
  the two profiles are of different devices: /device:TPU:8 before, /device:TPU:2 now
where the time goes in v5:
time: 60 us; the launch traced here: 59.7 us
  blocking collectives  33.9 us (56%)
  starting transfers between devices  16 us (27%)
  Pallas kernels  6.1 us (10%)
  waiting for transfers between devices  1.62 us (3%)
  local copies, waits for them, and re-layouts  1.33 us (2%)
  between operations  0.72 us (1%)
    all_to_all x2, blocking collectives, sent_to_all(): lax.all_to_all(copies, axis, split_axis=0, concat_axis=0, tiled=True, axi...  33.9 us
    ppermute x3, starting transfers between devices, passed_along(): return lax.ppermute(block, axis, route)  8.27 us
    all_to_all x1, starting transfers between devices, sent_to_all(): lax.all_to_all(copies, axis, split_axis=0, concat_axis=0, tiled=True, axi...  7.69 us
    pallas_call x7, Pallas kernels, call(): pl.pallas_call(kernel, out_shape=outs, in_specs=[SMEM] * scalars + [VMEM]...  4.61 us
    all_to_all x1, waiting for transfers between devices, sent_to_all(): lax.all_to_all(copies, axis, split_axis=0, concat_axis=0, tiled=True, axi...  1.61 us
    pallas_call x1, Pallas kernels, on_device(): pl.pallas_call(early_kernel, out_shape=(own_block,) * 3 + (kept(tiles, f3...  1.5 us
    unnamed x4, local copies, waits for them, and re-layouts  1.33 us
  transfers between devices with their start and end apart: 4, of which 1 were waited for; matrix products, arithmetic and copies ran while one was open for 0% of the time, Pallas kernels for 6%

profile of v5, /device:TPU:2, one launch (start us, length us, event | category | flops | bytes accessed | tf_op | source)
XLA Modules:
  0.0 59.7 jit_solution(10179690659806098083)
XLA Ops:
  0.6 3.5 %collective-permute-start = (bf16[256,256]{1,0:T(8,128)(2,1)}, bf16[256,256]{1,0:T(8,128)(2,1)S(1)}, u32[]{:S(2)}, u32[]{:S(2)}) collective-permute-start(bf16[256,256]{1,0:T(8,128)(2,1)} %bitcast.10), channel_id=1, source_target_pairs={{0,8},{8,16},{16,24},{24,32},{32,40},{40,48},{48,56},{56,64},{64,7... | collective-permute-start | bytes 393224 | tf_op jit(solution)/shard_map/ppermute | solution.py:49
  4.1 3.5 %collective-permute-start.1 = (bf16[256,256]{1,0:T(8,128)(2,1)}, bf16[256,256]{1,0:T(8,128)(2,1)S(1)}, u32[]{:S(2)}, u32[]{:S(2)}) collective-permute-start(bf16[256,256]{1,0:T(8,128)(2,1)} %bitcast.12), channel_id=1, source_target_pairs={{0,8},{8,16},{16,24},{24,32},{32,40},{40,48},{48,56},{56,64},{64,7... | collective-permute-start | bytes 393224 | tf_op jit(solution)/shard_map/ppermute | solution.py:49
  7.6 0.0 copy-start.1
  7.6 0.6 %copy-done.1 = bf16[256]{0:T(256)(128)(2,1)S(1)} copy-done((bf16[256]{0:T(256)(128)(2,1)S(1)}, bf16[256]{0:T(256)(128)(2,1)}, u32[]{:S(2)}) %copy-start.1) | copy-done | bytes 536
  8.3 0.0 copy-start
  8.3 0.7 %copy-done = bf16[2,320]{1,0:T(2,128)(2,1)S(1)} copy-done((bf16[2,320]{1,0:T(2,128)(2,1)S(1)}, bf16[2,320]{1,0:T(2,128)(2,1)}, u32[]{:S(2)}) %copy-start) | copy-done | bytes 1304
  9.0 1.5 %shard_map.93 = (bf16[256,256]{1,0:T(8,128)(2,1)S(1)}, bf16[256,256]{1,0:T(8,128)(2,1)S(1)}, bf16[256,256]{1,0:T(8,128)(2,1)S(1)}, f32[2,2,128,384]{3,2,1,0:T(8,...) custom-call(s32[1]{0:T(128)} %bitcast.first_ref, ...), custom_call_target="tpu_custom_call" | custom-call | tf_op jit(solution)/shard_map/pallas_call | solution.py:334
  10.5 0.0 collective-permute-done.prior_key_ref
  10.5 0.4 shard_map.94
  10.9 0.0 collective-permute-done.1.prior_value_ref
  10.9 0.4 shard_map.95
  11.3 11.3 %all_to_all.15.stat_ref = f32[8,4,128]{2,1,0:T(4,128)S(1)} all-to-all(f32[8,4,128]{2,1,0:T(4,128)S(1)} %get-tuple-element.33), channel_id=1, replica_groups={{5,0,1,2,3,4,6,7},{13,8,9,10,11,12,14,15},{21,16,17,18,19,20,22,23},{29..., dimensions={0} | all-to-all | bytes 32768 | tf_op jit(solution)/shard_map/all_to_all | solution.py:57
  22.6 1.1 %shard_map.96 = (bf16[256,256]{1,0:T(8,128)(2,1)S(1)}, bf16[2,2,128,384]{3,2,1,0:T(8,128)(2,1)S(1)}, f32[12,2,320]{2,1,0:T(2,128)S(1)}) custom-call(bf16[256,256]{1,0:T(8,128)(2,1)S(1)} %get-tuple-element.29.v_ref, bf16[256,256]{1,0:T(8,128)(2,1)S(1)} %collective-permute-done.1.prior_value_ref, f32[256,256]{1,0:T(8,128)S(1)} %get-tuple-element.30.scaled_ref, ...), custom_call_target="tpu_custom_call" | custom-call | tf_op jit(solution)/shard_map/pallas_call | solution.py:313
  23.7 0.3 shard_map.98
  24.0 1.3 %collective-permute-start.2 = (bf16[512,256]{1,0:T(8,128)(2,1)S(1)}, bf16[512,256]{1,0:T(8,128)(2,1)S(1)}, u32[]{:S(2)}, u32[]{:S(2)}) collective-permute-start(bf16[512,256]{1,0:T(8,128)(2,1)S(1)} %shard_map.98), channel_id=1, source_target_pairs={{8,0},{16,8},{24,16},{32,24},{40,32},{48,40},{56,48},{64,56},{72,6... | collective-permute-start | bytes 786440 | tf_op jit(solution)/shard_map/ppermute | solution.py:49
  25.3 22.7 %all_to_all.16.all_ref = f32[12,2,320]{2,1,0:T(2,128)S(1)} all-to-all(f32[12,2,320]{2,1,0:T(2,128)S(1)} %get-tuple-element.39), channel_id=1, replica_groups={{512,0,64,128,192,256,320,384,448,576,640,704},{520,8,72,136,200,264,32..., dimensions={0} | all-to-all | bytes 61440 | tf_op jit(solution)/shard_map/all_to_all | solution.py:57
  47.9 0.6 %shard_map.99 = f32[8,2,320]{2,1,0:T(2,128)} custom-call(f32[12,2,320]{2,1,0:T(2,128)S(1)} %all_to_all.16.all_ref), custom_call_target="tpu_custom_call" | custom-call | tf_op jit(solution)/shard_map/pallas_call | solution.py:313
  48.6 7.7 %all-to-all-start.2 = ((f32[8,2,320]{2,1,0:T(2,128)}), f32[8,2,320]{2,1,0:T(2,128)S(1)}, u32[]{:S(2)}, u32[]{:S(2)}) async-start(f32[8,2,320]{2,1,0:T(2,128)} %shard_map.99), calls=%async_computation.2 | async-start | bytes 49152 | tf_op jit(solution)/shard_map/all_to_all | solution.py:57
  56.3 1.0 %shard_map.97 = (bf16[256,256]{1,0:T(8,128)(2,1)}, f32[256,256]{1,0:T(8,128)S(1)}, f32[256,256]{1,0:T(8,128)S(1)}) custom-call(bf16[256,256]{1,0:T(8,128)(2,1)S(1)} %get-tuple-element.24.q_ref, bf16[256,256]{1,0:T(8,128)(2,1)S(1)} %get-tuple-element.25.k_ref, bf16[256,256]{1,0:T(8,128)(2,1)S(1)} %collective-permute-done.prior_key_ref, ...), custom_call_target="tpu_custom_call" | custom-call | tf_op jit(solution)/shard_map/pallas_call | solution.py:313
  57.2 1.6 %all-to-all-done.2.all_ref = f32[8,2,320]{2,1,0:T(2,128)S(1)} async-done(((f32[8,2,320]{2,1,0:T(2,128)}), f32[8,2,320]{2,1,0:T(2,128)S(1)}, u32[]{:S(2)}, u32[]{:S(2)}) %all-to-all-start.2) | async-done | bytes 20512 | tf_op jit(solution)/shard_map/all_to_all | solution.py:57
  58.8 0.0 collective-permute-done.2.back_ref
  58.8 0.8 %shard_map.100 = (bf16[256,256]{1,0:T(8,128)(2,1)}, bf16[256,256]{1,0:T(8,128)(2,1)}, f32[2,320]{1,0:T(2,128)}) custom-call(f32[256,256]{1,0:T(8,128)S(1)} %get-tuple-element.37.dk_ref, f32[256,256]{1,0:T(8,128)S(1)} %get-tuple-element.38.dv_ref, bf16[512,256]{1,0:T(8,128)(2,1)S(1)} %collective-permute-done.2.back_ref, ...), custom_call_target="tpu_custom_call" | custom-call | tf_op jit(solution)/shard_map/pallas_call | solution.py:313
  (1 shorter events, 0.0 us)
Async XLA Ops:
  0.6 9.9 %collective-permute-start = (bf16[256,256]{1,0:T(8,128)(2,1)}, bf16[256,256]{1,0:T(8,128)(2,1)S(1)}, u32[]{:S(2)}, u32[]{:S(2)}) collective-permute-start(bf16[256,256]{1,0:T(8,128)(2,1)} %bitcast.10), channel_id=1, source_target_pairs={{0,8},{8,16},{16,24},{24,32},{32,40},{40,48},{48,56},{56,64},{64,7... | collective-permute-start | bytes 393224 | tf_op jit(solution)/shard_map/ppermute | solution.py:49
  4.1 6.8 %collective-permute-start.1 = (bf16[256,256]{1,0:T(8,128)(2,1)}, bf16[256,256]{1,0:T(8,128)(2,1)S(1)}, u32[]{:S(2)}, u32[]{:S(2)}) collective-permute-start(bf16[256,256]{1,0:T(8,128)(2,1)} %bitcast.12), channel_id=1, source_target_pairs={{0,8},{8,16},{16,24},{24,32},{32,40},{40,48},{48,56},{56,64},{64,7... | collective-permute-start | bytes 393224 | tf_op jit(solution)/shard_map/ppermute | solution.py:49
  7.6 0.7 %copy-start.1 = (bf16[256]{0:T(256)(128)(2,1)S(1)}, bf16[256]{0:T(256)(128)(2,1)}, u32[]{:S(2)}) copy-start(bf16[256]{0:T(256)(128)(2,1)} %param.10) | copy-start | bytes 1540
  8.3 0.7 %copy-start = (bf16[2,320]{1,0:T(2,128)(2,1)S(1)}, bf16[2,320]{1,0:T(2,128)(2,1)}, u32[]{:S(2)}) copy-start(bf16[2,320]{1,0:T(2,128)(2,1)} %rel_ref.1) | copy-start | bytes 3844
  24.0 34.9 %collective-permute-start.2 = (bf16[512,256]{1,0:T(8,128)(2,1)S(1)}, bf16[512,256]{1,0:T(8,128)(2,1)S(1)}, u32[]{:S(2)}, u32[]{:S(2)}) collective-permute-start(bf16[512,256]{1,0:T(8,128)(2,1)S(1)} %shard_map.98), channel_id=1, source_target_pairs={{8,0},{16,8},{24,16},{32,24},{40,32},{48,40},{56,48},{64,56},{72,6... | collective-permute-start | bytes 786440 | tf_op jit(solution)/shard_map/ppermute | solution.py:49
  48.6 10.3 %all-to-all-start.2 = ((f32[8,2,320]{2,1,0:T(2,128)}), f32[8,2,320]{2,1,0:T(2,128)S(1)}, u32[]{:S(2)}, u32[]{:S(2)}) async-start(f32[8,2,320]{2,1,0:T(2,128)} %shard_map.99), calls=%async_computation.2 | async-start | bytes 49152 | tf_op jit(solution)/shard_map/all_to_all | solution.py:57

commit v6 on v5

--- a/solution.py
+++ b/solution.py
@@ -286,14 +286,34 @@
                 own_ref[rows_of(g), ch] = total * factor
 
 
-def final_kernel(dk_ref, dv_ref, back_ref, all_ref, turn_ref, key_ref, value_ref, table_ref):
+def final_kernel(
+    dk_ref,
+    dv_ref,
+    back_ref,
+    all_ref,
+    turn_ref,
+    key_hbm,
+    value_hbm,
+    table_hbm,
+    key_ref,
+    value_ref,
+    table_ref,
+    sems,
+):
     rows = dk_ref.shape[0]
     heads = table_ref.shape[0]
+    moves = ((key_ref, key_hbm), (value_ref, value_hbm), (table_ref, table_hbm))
+    copies = [pltpu.make_async_copy(a, b, sems.at[i]) for i, (a, b) in enumerate(moves)]
     key_ref[...] = (dk_ref[...] + back_ref[:rows].astype(f32)).astype(bf16)
+    copies[0].start()
     value_ref[...] = (dv_ref[...] + back_ref[rows:].astype(f32)).astype(bf16)
+    copies[1].start()
     pieces = jnp.concatenate(parts_of(jnp.sum(all_ref[...], axis=0), 3), axis=0)
     lines = dot(pieces, turn_ref[...], ((1,), (0,)))
     table_ref[...] = lines[2 * heads :] + lines[heads : 2 * heads] + lines[:heads]
+    copies[2].start()
+    for copy in copies:
+        copy.wait()
 
 
 def relay_kernel(all_ref, out_ref):
@@ -370,11 +390,23 @@
         (out((rows, width), bf16), kept((rows, width), f32), kept((rows, width), f32)),
         *(q, k, prior_keys, weight, grad, low),
     )
-    grad_keys, grad_values, grad_table = call(
+    grad_keys, grad_values, grad_table = pl.pallas_call(
         final_kernel,
-        (out((rows, width), bf16), out((rows, width), bf16), out((heads, REL), f32)),
-        *(dk, dv, back, table, turn),
-    )
+        out_shape=(
+            pltpu.HBM((rows, width), bf16),
+            pltpu.HBM((rows, width), bf16),
+            pltpu.HBM((heads, REL), f32),
+        ),
+        in_specs=[VMEM] * 5,
+        out_specs=(HBM,) * 3,
+        scratch_shapes=[
+            pltpu.VMEM((rows, width), bf16),
+            pltpu.VMEM((rows, width), bf16),
+            pltpu.VMEM((heads, REL), f32),
+            pltpu.SemaphoreType.DMA((3,)),
+        ],
+        compiler_params=pltpu.CompilerParams(vmem_limit_bytes=ROOM),
+    )(*(near(a) for a in (dk, dv, back, table, turn)))
     return (dq.reshape(shape), grad_keys.reshape(shape), grad_values.reshape(shape), grad_table)
 
 

time: 60 us -> 60 us (level)
    pallas_call x0 -> x1, Pallas kernels: none -> 0.84 us  [on_device(): pl.pallas_call(final_kernel, out_shape=(pltpu.HBM((rows, width), bf16), p...]
    pallas_call x7 -> x6, Pallas kernels: 4.61 us -> 3.78 us  [call(): pl.pallas_call(kernel, out_shape=outs, in_specs=[SMEM] * scalars + [VMEM]...]
where the time goes in v6:
time: 60 us; the launch traced here: 59.7 us
  blocking collectives  33.9 us (56%)
  starting transfers between devices  16 us (27%)
  Pallas kernels  6.12 us (10%)
  waiting for transfers between devices  1.62 us (3%)
  local copies, waits for them, and re-layouts  1.33 us (2%)
  between operations  0.72 us (1%)
    all_to_all x2, blocking collectives, sent_to_all(): lax.all_to_all(copies, axis, split_axis=0, concat_axis=0, tiled=True, axi...  33.9 us
    ppermute x3, starting transfers between devices, passed_along(): return lax.ppermute(block, axis, route)  8.27 us
    all_to_all x1, starting transfers between devices, sent_to_all(): lax.all_to_all(copies, axis, split_axis=0, concat_axis=0, tiled=True, axi...  7.69 us
    pallas_call x6, Pallas kernels, call(): pl.pallas_call(kernel, out_shape=outs, in_specs=[SMEM] * scalars + [VMEM]...  3.78 us
    all_to_all x1, waiting for transfers between devices, sent_to_all(): lax.all_to_all(copies, axis, split_axis=0, concat_axis=0, tiled=True, axi...  1.61 us
    pallas_call x1, Pallas kernels, on_device(): pl.pallas_call(early_kernel, out_shape=(own_block,) * 3 + (kept(tiles, f3...  1.5 us
    unnamed x4, local copies, waits for them, and re-layouts  1.33 us
  transfers between devices with their start and end apart: 4, of which 1 were waited for; matrix products, arithmetic and copies ran while one was open for 0% of the time, Pallas kernels for 6%

profile of v6, /device:TPU:2, one launch (start us, length us, event | category | flops | bytes accessed | tf_op | source)
XLA Modules:
  0.0 59.7 jit_solution(2560082657591935036)
XLA Ops:
  0.6 3.5 %collective-permute-start = (bf16[256,256]{1,0:T(8,128)(2,1)}, bf16[256,256]{1,0:T(8,128)(2,1)S(1)}, u32[]{:S(2)}, u32[]{:S(2)}) collective-permute-start(bf16[256,256]{1,0:T(8,128)(2,1)} %bitcast.10), channel_id=1, source_target_pairs={{0,8},{8,16},{16,24},{24,32},{32,40},{40,48},{48,56},{56,64},{64,7... | collective-permute-start | bytes 393224 | tf_op jit(solution)/shard_map/ppermute | solution.py:49
  4.1 3.5 %collective-permute-start.1 = (bf16[256,256]{1,0:T(8,128)(2,1)}, bf16[256,256]{1,0:T(8,128)(2,1)S(1)}, u32[]{:S(2)}, u32[]{:S(2)}) collective-permute-start(bf16[256,256]{1,0:T(8,128)(2,1)} %bitcast.12), channel_id=1, source_target_pairs={{0,8},{8,16},{16,24},{24,32},{32,40},{40,48},{48,56},{56,64},{64,7... | collective-permute-start | bytes 393224 | tf_op jit(solution)/shard_map/ppermute | solution.py:49
  7.6 0.0 copy-start.1
  7.6 0.6 %copy-done.1 = bf16[256]{0:T(256)(128)(2,1)S(1)} copy-done((bf16[256]{0:T(256)(128)(2,1)S(1)}, bf16[256]{0:T(256)(128)(2,1)}, u32[]{:S(2)}) %copy-start.1) | copy-done | bytes 536
  8.3 0.0 copy-start
  8.3 0.7 %copy-done = bf16[2,320]{1,0:T(2,128)(2,1)S(1)} copy-done((bf16[2,320]{1,0:T(2,128)(2,1)S(1)}, bf16[2,320]{1,0:T(2,128)(2,1)}, u32[]{:S(2)}) %copy-start) | copy-done | bytes 1304
  9.0 1.5 %shard_map.93 = (bf16[256,256]{1,0:T(8,128)(2,1)S(1)}, bf16[256,256]{1,0:T(8,128)(2,1)S(1)}, bf16[256,256]{1,0:T(8,128)(2,1)S(1)}, f32[2,2,128,384]{3,2,1,0:T(8,...) custom-call(s32[1]{0:T(128)} %bitcast.first_ref, ...), custom_call_target="tpu_custom_call" | custom-call | tf_op jit(solution)/shard_map/pallas_call | solution.py:354
  10.5 0.0 collective-permute-done.prior_key_ref
  10.5 0.4 shard_map.94
  10.9 0.0 collective-permute-done.1.prior_value_ref
  10.9 0.4 shard_map.95
  11.3 11.3 %all_to_all.15.stat_ref = f32[8,4,128]{2,1,0:T(4,128)S(1)} all-to-all(f32[8,4,128]{2,1,0:T(4,128)S(1)} %get-tuple-element.33), channel_id=1, replica_groups={{5,0,1,2,3,4,6,7},{13,8,9,10,11,12,14,15},{21,16,17,18,19,20,22,23},{29..., dimensions={0} | all-to-all | bytes 32768 | tf_op jit(solution)/shard_map/all_to_all | solution.py:57
  22.6 1.1 %shard_map.96 = (bf16[256,256]{1,0:T(8,128)(2,1)S(1)}, bf16[2,2,128,384]{3,2,1,0:T(8,128)(2,1)S(1)}, f32[12,2,320]{2,1,0:T(2,128)S(1)}) custom-call(bf16[256,256]{1,0:T(8,128)(2,1)S(1)} %get-tuple-element.29.v_ref, bf16[256,256]{1,0:T(8,128)(2,1)S(1)} %collective-permute-done.1.prior_value_ref, f32[256,256]{1,0:T(8,128)S(1)} %get-tuple-element.30.scaled_ref, ...), custom_call_target="tpu_custom_call" | custom-call | tf_op jit(solution)/shard_map/pallas_call | solution.py:333
  23.7 0.3 shard_map.98
  24.0 1.3 %collective-permute-start.2 = (bf16[512,256]{1,0:T(8,128)(2,1)S(1)}, bf16[512,256]{1,0:T(8,128)(2,1)S(1)}, u32[]{:S(2)}, u32[]{:S(2)}) collective-permute-start(bf16[512,256]{1,0:T(8,128)(2,1)S(1)} %shard_map.98), channel_id=1, source_target_pairs={{8,0},{16,8},{24,16},{32,24},{40,32},{48,40},{56,48},{64,56},{72,6... | collective-permute-start | bytes 786440 | tf_op jit(solution)/shard_map/ppermute | solution.py:49
  25.3 22.7 %all_to_all.16.all_ref = f32[12,2,320]{2,1,0:T(2,128)S(1)} all-to-all(f32[12,2,320]{2,1,0:T(2,128)S(1)} %get-tuple-element.39), channel_id=1, replica_groups={{512,0,64,128,192,256,320,384,448,576,640,704},{520,8,72,136,200,264,32..., dimensions={0} | all-to-all | bytes 61440 | tf_op jit(solution)/shard_map/all_to_all | solution.py:57
  47.9 0.6 %shard_map.99 = f32[8,2,320]{2,1,0:T(2,128)} custom-call(f32[12,2,320]{2,1,0:T(2,128)S(1)} %all_to_all.16.all_ref), custom_call_target="tpu_custom_call" | custom-call | tf_op jit(solution)/shard_map/pallas_call | solution.py:333
  48.6 7.7 %all-to-all-start.2 = ((f32[8,2,320]{2,1,0:T(2,128)}), f32[8,2,320]{2,1,0:T(2,128)S(1)}, u32[]{:S(2)}, u32[]{:S(2)}) async-start(f32[8,2,320]{2,1,0:T(2,128)} %shard_map.99), calls=%async_computation.2 | async-start | bytes 49152 | tf_op jit(solution)/shard_map/all_to_all | solution.py:57
  56.3 1.0 %shard_map.97 = (bf16[256,256]{1,0:T(8,128)(2,1)}, f32[256,256]{1,0:T(8,128)S(1)}, f32[256,256]{1,0:T(8,128)S(1)}) custom-call(bf16[256,256]{1,0:T(8,128)(2,1)S(1)} %get-tuple-element.24.q_ref, bf16[256,256]{1,0:T(8,128)(2,1)S(1)} %get-tuple-element.25.k_ref, bf16[256,256]{1,0:T(8,128)(2,1)S(1)} %collective-permute-done.prior_key_ref, ...), custom_call_target="tpu_custom_call" | custom-call | tf_op jit(solution)/shard_map/pallas_call | solution.py:333
  57.2 1.6 %all-to-all-done.2.all_ref = f32[8,2,320]{2,1,0:T(2,128)S(1)} async-done(((f32[8,2,320]{2,1,0:T(2,128)}), f32[8,2,320]{2,1,0:T(2,128)S(1)}, u32[]{:S(2)}, u32[]{:S(2)}) %all-to-all-start.2) | async-done | bytes 20512 | tf_op jit(solution)/shard_map/all_to_all | solution.py:57
  58.8 0.0 collective-permute-done.2.back_ref
  58.8 0.8 %shard_map.100 = (bf16[256,256]{1,0:T(8,128)(2,1)}, bf16[256,256]{1,0:T(8,128)(2,1)}, f32[2,320]{1,0:T(2,128)}) custom-call(f32[256,256]{1,0:T(8,128)S(1)} %get-tuple-element.37.dk_ref, f32[256,256]{1,0:T(8,128)S(1)} %get-tuple-element.38.dv_ref, bf16[512,256]{1,0:T(8,128)(2,1)S(1)} %collective-permute-done.2.back_ref, ...), custom_call_target="tpu_custom_call" | custom-call | tf_op jit(solution)/shard_map/pallas_call | solution.py:393
  (1 shorter events, 0.0 us)
Async XLA Ops:
  0.6 9.9 %collective-permute-start = (bf16[256,256]{1,0:T(8,128)(2,1)}, bf16[256,256]{1,0:T(8,128)(2,1)S(1)}, u32[]{:S(2)}, u32[]{:S(2)}) collective-permute-start(bf16[256,256]{1,0:T(8,128)(2,1)} %bitcast.10), channel_id=1, source_target_pairs={{0,8},{8,16},{16,24},{24,32},{32,40},{40,48},{48,56},{56,64},{64,7... | collective-permute-start | bytes 393224 | tf_op jit(solution)/shard_map/ppermute | solution.py:49
  4.1 6.8 %collective-permute-start.1 = (bf16[256,256]{1,0:T(8,128)(2,1)}, bf16[256,256]{1,0:T(8,128)(2,1)S(1)}, u32[]{:S(2)}, u32[]{:S(2)}) collective-permute-start(bf16[256,256]{1,0:T(8,128)(2,1)} %bitcast.12), channel_id=1, source_target_pairs={{0,8},{8,16},{16,24},{24,32},{32,40},{40,48},{48,56},{56,64},{64,7... | collective-permute-start | bytes 393224 | tf_op jit(solution)/shard_map/ppermute | solution.py:49
  7.6 0.7 %copy-start.1 = (bf16[256]{0:T(256)(128)(2,1)S(1)}, bf16[256]{0:T(256)(128)(2,1)}, u32[]{:S(2)}) copy-start(bf16[256]{0:T(256)(128)(2,1)} %param.10) | copy-start | bytes 1540
  8.3 0.7 %copy-start = (bf16[2,320]{1,0:T(2,128)(2,1)S(1)}, bf16[2,320]{1,0:T(2,128)(2,1)}, u32[]{:S(2)}) copy-start(bf16[2,320]{1,0:T(2,128)(2,1)} %rel_ref.1) | copy-start | bytes 3844
  24.0 34.9 %collective-permute-start.2 = (bf16[512,256]{1,0:T(8,128)(2,1)S(1)}, bf16[512,256]{1,0:T(8,128)(2,1)S(1)}, u32[]{:S(2)}, u32[]{:S(2)}) collective-permute-start(bf16[512,256]{1,0:T(8,128)(2,1)S(1)} %shard_map.98), channel_id=1, source_target_pairs={{8,0},{16,8},{24,16},{32,24},{40,32},{48,40},{56,48},{64,56},{72,6... | collective-permute-start | bytes 786440 | tf_op jit(solution)/shard_map/ppermute | solution.py:49
  48.6 10.3 %all-to-all-start.2 = ((f32[8,2,320]{2,1,0:T(2,128)}), f32[8,2,320]{2,1,0:T(2,128)S(1)}, u32[]{:S(2)}, u32[]{:S(2)}) async-start(f32[8,2,320]{2,1,0:T(2,128)} %shard_map.99), calls=%async_computation.2 | async-start | bytes 49152 | tf_op jit(solution)/shard_map/all_to_all | solution.py:57
